TPU v7x, 32 devices: a whole 2x2x4 slice. The times are simulated.
32 devices in a mesh: grp: 2 (over y), sp: 8 (over z, core), tp: 2 (over x).
Axes of the slice: x: 2, y: 2, z: 4, core: 2. Of those that a mesh axis runs over, the one named last changes fastest.
Arguments:
- query_plain: bfloat16 [2560, 1024], P(('grp', 'sp'), 'tp'), parts along dimension 0, may hold values from -6 to 6
- query_turn: bfloat16 [2560, 512], P(('grp', 'sp'), 'tp'), parts along dimension 0, may hold values from -40 to 40, as said below
- latent: bfloat16 [2560, 512], P(('grp', 'sp')), parts along dimension 0, may hold values from -6 to 6
- key_turn: bfloat16 [2560, 64], P(('grp', 'sp')), parts along dimension 0, may hold values from -40 to 40, as said below
- latent_norm_scale: bfloat16 [512], replicated, may hold values from 0.099609375 to 1.8984375
- plain_key_matrix: bfloat16 [512, 1024], P(None, 'tp'), may hold values from -0.25 to 0.25
- value_matrix: bfloat16 [512, 1024], P(None, 'tp'), may hold values from -0.25 to 0.25
- residual: bfloat16 [2560, 2048], P(('grp', 'sp', 'tp')), parts along dimension 0, may hold values from -6 to 6
- out_weight: bfloat16 [1024, 2048], replicated, may hold values from -6 to 6
- ffn_gain: bfloat16 [2048], replicated, may hold values from 0.099609375 to 1.8984375
- gate_weight: bfloat16 [8, 2048, 1024], P('sp', None, 'tp'), may hold values from -1 to 1
- up_weight: bfloat16 [8, 2048, 1024], P('sp', None, 'tp'), may hold values from -1 to 1
- down_weight: bfloat16 [8, 1024, 2048], P('sp', 'tp'), may hold values from -0.0625 to 0.0625
- routes: int32 [2560, 4], P(('grp', 'sp', 'tp')), parts along dimension 0, may hold values from 0 to 7, all different within a row; in each aligned block of 80 rows (0 to 79, 80 to 159, ...) at most 60 rows name the same one
- route_weights: float32 [2560, 4], P(('grp', 'sp', 'tp')), parts along dimension 0, may hold values from 0.1 to 0.6
Outputs:
- mixed: bfloat16 [2560, 2048], P(('grp', 'sp', 'tp')), parts along dimension 0
There are 2 independent parts, one for each index of `grp`. A program takes and returns all parts, laid end to end along the dimension named above; an argument that names none is the same for every part. Nothing has to cross between parts.
Inputs may be any that keep to these rules, and one draw needn't show every extreme that they name: `query_turn`: in the hidden draw some rows are large. `key_turn`: in the hidden draw some rows are large. `routes`: each row names 4 different experts. In each aligned block of 80 rows (the rows of one device) no expert is named more than 60 times, a bound that some block reaches.
All inputs are finite; a program needn't handle non-finite values.
Results may differ from a plain program's by a relative error of at most 0.015.
Values may be sent and summed in bfloat16 or wider, within the bound.
A program may use at most 128 MiB of HBM per device.

v0:
```python
import functools

import jax
import jax.numpy as jnp
from jax import lax
from jax.experimental import pallas as pl
from jax.experimental.pallas import tpu as pltpu
from jax.sharding import PartitionSpec as P

PLAIN_HEAD_WIDTH = 128
QK_ROPE = 64
VALUE_WIDTH = 128
GRID_W = 64


theta = 10000.0
eps = 1e-06
limit = 7.0
slope = 1.702
CORES = 2
STRIPS = 2
VMEM_BYTES = 60 * 2**20


def turn(vector, row_shift, col_shift):
    width = vector.shape[-1]
    count = width // 4
    half = width // 2
    freqs = theta ** (-jnp.arange(count, dtype=jnp.float32) / count)
    extra = (1,) * (vector.ndim - 2)
    pieces = []
    for portion, shift in ((vector[..., :half], row_shift), (vector[..., half:], col_shift)):
        angle = (shift.astype(jnp.float32)[:, None] * freqs[None, :]).reshape(
            (shift.shape[0],) + extra + (count,)
        )
        lower = portion[..., :count]
        upper = portion[..., count:]
        pieces.append(
            jnp.concatenate(
                [
                    lower * jnp.cos(angle) - upper * jnp.sin(angle),
                    lower * jnp.sin(angle) + upper * jnp.cos(angle),
                ],
                axis=-1,
            )
        )
    return jnp.concatenate(pieces, axis=-1)


def norm_scale(values, gain):
    wide = values.astype(jnp.float32)
    return (
        wide
        * lax.rsqrt(jnp.mean(wide * wide, axis=-1, keepdims=True) + eps)
        * gain.astype(jnp.float32)
    )


def expert_active(rows, gate_w, up_w):
    gate_pre = jnp.minimum(jnp.dot(rows, gate_w, preferred_element_type=jnp.float32), limit)
    up_pre = jnp.clip(jnp.dot(rows, up_w, preferred_element_type=jnp.float32), -limit, limit)
    return ((up_pre + 1.0) * gate_pre * jax.nn.sigmoid(slope * gate_pre)).astype(jnp.bfloat16)


def flipped(index, mask):
    out = index
    bit = 1
    while bit <= mask:
        if mask & bit:
            out = out + bit - 2 * bit * ((index // bit) % 2)
        bit *= 2
    return out


def gatherer(chips, group, own, gathered, sems, launch):
    z_send, z_recv, x_send, x_recv, c_send, c_recv = sems
    place = lax.axis_index("sp")
    column = lax.axis_index("tp")
    chip, core = place // CORES, place % CORES
    per_chip = CORES * group
    partner = {"sp": chip * CORES + 1 - core}

    def other(shift):
        return (column + shift) % group

    def slot(k, core_at, column_at):
        return flipped(chip, k) * per_chip + core_at * group + column_at

    def chip_peer(k):
        return {"sp": flipped(chip, k) * CORES + core}

    def remote(src, dst, send_sem, recv_sem, device):
        return pltpu.make_async_remote_copy(
            src_ref=src, dst_ref=dst, send_sem=send_sem, recv_sem=recv_sem, device_id=device
        )

    def greet():
        barrier = pltpu.get_barrier_semaphore()
        pl.semaphore_signal(barrier, inc=1, device_id=partner)
        for k in range(1, chips):
            pl.semaphore_signal(barrier, inc=1, device_id=chip_peer(k))
        for shift in range(1, group):
            pl.semaphore_signal(barrier, inc=1, device_id={"tp": other(shift)})

    def met():
        pl.semaphore_wait(pltpu.get_barrier_semaphore(), chips + group - 1)

    def source(k, back):
        if k == 0 and back == 0:
            return own
        return gathered.at[slot(k, core, other(group - back))]

    def chip_wait(k):
        landed = gathered.at[slot(k, core, column)]
        remote(landed, landed, z_send.at[k], z_recv.at[k], chip_peer(k)).wait_recv()

    def core_copy(k, back):
        return remote(
            source(k, back),
            gathered.at[slot(k, core, other(group - back))],
            c_send.at[k, back],
            c_recv.at[k, back],
            partner,
        )

    def core_wait(k, back):
        landed = gathered.at[slot(k, 1 - core, other(group - back))]
        remote(landed, landed, c_send.at[k, back], c_recv.at[k, back], partner).wait_recv()

    def tp_copy(k, shift):
        return remote(
            source(k, 0),
            gathered.at[slot(k, core, column)],
            x_send.at[k, shift],
            x_recv.at[k, shift],
            {"tp": other(shift)},
        )

    def tp_wait(k, shift):
        landed = gathered.at[slot(k, core, other(group - shift))]
        remote(
            landed, landed, x_send.at[k, shift], x_recv.at[k, shift], {"tp": other(shift)}
        ).wait_recv()

    def spread(k):
        for shift in range(1, group):
            launch(tp_copy(k, shift))
        launch(core_copy(k, 0))

    def begin():
        for k in range(1, chips):
            launch(
                remote(
                    own,
                    gathered.at[slot(0, core, column)],
                    z_send.at[k],
                    z_recv.at[k],
                    chip_peer(k),
                )
            )
        spread(0)

    def step(k):
        if k + 1 < chips:
            chip_wait(k + 1)
            spread(k + 1)
        for shift in range(1, group):
            tp_wait(k, shift)
            launch(core_copy(k, shift))
        for back in range(group):
            core_wait(k, back)

    return greet, met, begin, step, slot, chip_peer, partner, other, remote


def gather_kernel(chips, group, own, gathered, *sems):
    sends = []

    def launch(copy):
        copy.start()
        sends.append(copy)

    greet, met, begin, step, slot = gatherer(chips, group, own, gathered, sems, launch)[:5]
    greet()
    met()
    begin()
    gathered[slot(0, lax.axis_index("sp") % CORES, lax.axis_index("tp"))] = own[...]
    for k in range(chips):
        step(k)
    for copy in sends:
        copy.wait_send()


def gather_sems(chips, group):
    dma = pltpu.SemaphoreType.DMA
    return [dma((chips,))] * 2 + [dma((chips, group))] * 4


def run_gather(rows):
    group = lax.axis_size("tp")
    chips = lax.axis_size("sp") // CORES
    whole = pl.BlockSpec(memory_space=pltpu.VMEM)
    return pl.pallas_call(
        functools.partial(gather_kernel, chips, group),
        out_shape=jax.ShapeDtypeStruct((chips * CORES * group,) + rows.shape, rows.dtype),
        in_specs=[whole],
        out_specs=whole,
        scratch_shapes=gather_sems(chips, group),
        compiler_params=pltpu.CompilerParams(
            collective_id=1, has_side_effects=True, vmem_limit_bytes=VMEM_BYTES // 2
        ),
    )(rows)


def experts_kernel(
    chips,
    group,
    attended_ref,
    residual_ref,
    gain_ref,
    share_ref,
    out_hbm,
    gate_hbm,
    up_hbm,
    down_hbm,
    out_ref,
    heads,
    hidden,
    rows_ref,
    total_ref,
    gathered,
    partial,
    from_core,
    from_tp,
    from_chip,
    outw_ref,
    gate_ref,
    up_ref,
    down_ref,
    load_sem,
    h_send,
    h_recv,
    rc_send,
    rc_recv,
    rx_send,
    rx_recv,
    rz_send,
    rz_recv,
    *sems,
):
    column = lax.axis_index("tp")
    core = lax.axis_index("sp") % CORES
    rows_dev, model_width = rows_ref.shape
    per_chip = CORES * group
    sends = []

    def launch(copy):
        copy.start()
        sends.append(copy)

    greet, met, begin, step, slot, chip_peer, partner, other, remote = gatherer(
        chips, group, rows_ref, gathered, sems, launch
    )
    greet()
    loads = [
        pltpu.make_async_copy(src, dst, load_sem.at[i])
        for i, (src, dst) in enumerate(
            (
                (out_hbm, outw_ref),
                (gate_hbm, gate_ref),
                (up_hbm, up_ref),
                (down_hbm, down_ref),
            )
        )
    ]
    for load in loads:
        load.start()
    met()

    def heads_copy(shift):
        return remote(
            attended_ref.at[other(shift)],
            heads.at[column],
            h_send.at[shift],
            h_recv.at[shift],
            {"tp": other(shift)},
        )

    def heads_wait(shift):
        landed = heads.at[other(group - shift)]
        remote(
            landed, landed, h_send.at[shift], h_recv.at[shift], {"tp": other(shift)}
        ).wait_recv()

    for shift in range(1, group):
        launch(heads_copy(shift))
    heads[column] = attended_ref[column]
    loads[0].wait()
    for shift in range(1, group):
        heads_wait(shift)
    joined = jnp.concatenate([heads[at] for at in range(group)], axis=1)
    projected = jnp.dot(joined, outw_ref[...], preferred_element_type=jnp.float32)
    mixed = (residual_ref[...].astype(jnp.float32) + projected).astype(jnp.bfloat16)
    normed = norm_scale(mixed, gain_ref[...]).astype(jnp.bfloat16)
    rows_ref[...] = normed
    gathered[slot(0, core, column)] = normed
    hidden[...] = mixed
    begin()

    def compute(k):
        first = slot(k, 0, 0)
        rows = gathered[pl.ds(first, per_chip)].reshape(per_chip * rows_dev, model_width)
        active = expert_active(rows, gate_ref[...], up_ref[...])
        share = share_ref[pl.ds(first, per_chip)].reshape(per_chip * rows_dev, 1)
        product = jnp.dot(active, down_ref[...], preferred_element_type=jnp.float32)
        partial[pl.ds(first, per_chip)] = (
            (product * share).astype(jnp.bfloat16).reshape(per_chip, rows_dev, model_width)
        )

    def partner_copy(k):
        return remote(
            partial.at[pl.ds(slot(k, 1 - core, 0), group)],
            from_core.at[k],
            rc_send.at[k],
            rc_recv.at[k],
            partner,
        )

    strips = STRIPS if model_width % (128 * STRIPS) == 0 else 1
    strip = model_width // strips

    def part(at):
        return pl.ds(at * strip, strip)

    def tp_sum_copy(k, shift, at):
        return remote(
            partial.at[slot(k, core, other(shift)), :, part(at)],
            from_tp.at[k, shift - 1, :, part(at)],
            rx_send.at[k, shift, at],
            rx_recv.at[k, shift, at],
            {"tp": other(shift)},
        )

    def chip_sum_copy(k, at):
        return remote(
            partial.at[slot(k, core, column), :, part(at)],
            from_chip.at[k, :, part(at)],
            rz_send.at[k, at],
            rz_recv.at[k, at],
            chip_peer(k),
        )

    def sum_cores(k):
        partner_copy(k).wait_recv()
        first = slot(k, core, 0)
        partial[pl.ds(first, group)] = (
            partial[pl.ds(first, group)].astype(jnp.float32) + from_core[k].astype(jnp.float32)
        ).astype(jnp.bfloat16)
        for at in range(strips):
            for shift in range(1, group):
                launch(tp_sum_copy(k, shift, at))

    def sum_tp(k):
        for at in range(strips):
            total = partial[slot(k, core, column), :, part(at)].astype(jnp.float32)
            for shift in range(1, group):
                tp_sum_copy(k, shift, at).wait_recv()
                total = total + from_tp[k, shift - 1, :, part(at)].astype(jnp.float32)
            if k == 0:
                total_ref[:, part(at)] = hidden[:, part(at)].astype(jnp.float32) + total
            else:
                partial[slot(k, core, column), :, part(at)] = total.astype(jnp.bfloat16)
                launch(chip_sum_copy(k, at))

    for k in range(chips + 2):
        if k < chips:
            step(k)
            if k == 0:
                for load in loads[1:]:
                    load.wait()
            compute(k)
            launch(partner_copy(k))
        if 0 <= k - 1 < chips:
            sum_cores(k - 1)
        if 0 <= k - 2 < chips:
            sum_tp(k - 2)
    total = total_ref[...]
    for k in range(1, chips):
        for at in range(strips):
            chip_sum_copy(k, at).wait_recv()
        total = total + from_chip[k].astype(jnp.float32)
    out_ref[...] = total.astype(jnp.bfloat16)
    for copy in sends:
        copy.wait_send()


def run_experts(attended, residual, gain, shares, out_w, gate_w, up_w, down_w):
    group = lax.axis_size("tp")
    chips = lax.axis_size("sp") // CORES
    rows_dev, model_width = residual.shape
    blocks = chips * CORES * group
    dma = pltpu.SemaphoreType.DMA
    block = (rows_dev, model_width)
    heads = (group, rows_dev, attended.shape[1])
    whole = pl.BlockSpec(memory_space=pltpu.VMEM)
    return pl.pallas_call(
        functools.partial(experts_kernel, chips, group),
        out_shape=jax.ShapeDtypeStruct(block, jnp.bfloat16),
        in_specs=[whole] * 4 + [pl.BlockSpec(memory_space=pl.ANY)] * 4,
        out_specs=whole,
        scratch_shapes=[
            pltpu.VMEM(heads, jnp.bfloat16),
            pltpu.VMEM(block, jnp.bfloat16),
            pltpu.VMEM(block, jnp.bfloat16),
            pltpu.VMEM(block, jnp.float32),
            pltpu.VMEM((blocks,) + block, jnp.bfloat16),
            pltpu.VMEM((blocks,) + block, jnp.bfloat16),
            pltpu.VMEM((chips, group) + block, jnp.bfloat16),
            pltpu.VMEM((chips, group - 1) + block, jnp.bfloat16),
            pltpu.VMEM((chips,) + block, jnp.bfloat16),
            pltpu.VMEM(out_w.shape, jnp.bfloat16),
            pltpu.VMEM(gate_w.shape, jnp.bfloat16),
            pltpu.VMEM(up_w.shape, jnp.bfloat16),
            pltpu.VMEM(down_w.shape, jnp.bfloat16),
            dma((4,)),
            dma((group,)),
            dma((group,)),
            dma((chips,)),
            dma((chips,)),
            dma((chips, group, STRIPS)),
            dma((chips, group, STRIPS)),
            dma((chips, STRIPS)),
            dma((chips, STRIPS)),
        ]
        + gather_sems(chips, group),
        compiler_params=pltpu.CompilerParams(
            collective_id=0, has_side_effects=True, vmem_limit_bytes=VMEM_BYTES
        ),
    )(
        attended.reshape(heads),
        residual,
        gain.reshape(1, model_width),
        shares.reshape(blocks, rows_dev, 1),
        out_w,
        gate_w,
        up_w,
        down_w,
    )


def experts_fit(rows_dev, model_width):
    group, places = lax.axis_size("tp"), lax.axis_size("sp")
    chips = places // CORES
    if group < 2 or places % CORES or chips & (chips - 1) or rows_dev % 16:
        return False
    return 3 * places * group * rows_dev * model_width * 2 < VMEM_BYTES // 2


def on_device(
    query_plain,
    query_turn,
    latent,
    key_turn,
    latent_norm_scale,
    plain_key_matrix,
    value_matrix,
    residual,
    out_weight,
    ffn_gain,
    gate_weight,
    up_weight,
    down_weight,
    routes,
    route_weights,
):
    tok_dev = latent.shape[0]
    heads_dev = query_plain.shape[1] // PLAIN_HEAD_WIDTH
    model_width = residual.shape[1]
    place = lax.axis_index("sp") * tok_dev + jnp.arange(tok_dev, dtype=jnp.int32)
    grid_row = place // GRID_W
    grid_col = place % GRID_W
    rows_dev, model_width = residual.shape
    group = lax.axis_size("tp")
    count = lax.axis_size("sp")
    fits = experts_fit(rows_dev, model_width)
    expert_ids = jnp.arange(count, dtype=jnp.int32)
    share = jnp.sum(
        route_weights[..., None] * (routes[..., None] == expert_ids).astype(jnp.float32), axis=1
    )
    latent_width = latent.shape[1]
    wide = latent_width + QK_ROPE

    def key_side(latents, turns, at_row, at_col):
        normed_latent = norm_scale(latents, latent_norm_scale).astype(jnp.bfloat16)
        key_rot = turn(turns.astype(jnp.float32), at_row, at_col).astype(jnp.bfloat16)
        return [normed_latent, key_rot]

    if fits:
        first = lax.axis_index("tp") * rows_dev
        high = lax.reduce_precision(share, 8, 7)
        filled = wide + 2 * count
        sent = jnp.concatenate(
            key_side(
                lax.dynamic_slice_in_dim(latent, first, rows_dev, 0),
                lax.dynamic_slice_in_dim(key_turn, first, rows_dev, 0),
                lax.dynamic_slice_in_dim(grid_row, first, rows_dev, 0),
                lax.dynamic_slice_in_dim(grid_col, first, rows_dev, 0),
            )
            + [high.astype(jnp.bfloat16), (share - high).astype(jnp.bfloat16)]
            + [jnp.zeros((rows_dev, -filled % 128), jnp.bfloat16)],
            axis=1,
        )
        everyone = run_gather(sent)
        everyone = everyone.reshape(everyone.shape[0] * rows_dev, everyone.shape[2])
        shares = everyone[:, wide : wide + count].astype(jnp.float32) + everyone[
            :, wide + count : filled
        ].astype(jnp.float32)
    else:
        sent = jnp.concatenate(key_side(latent, key_turn, grid_row, grid_col), axis=1)
        everyone = lax.all_gather(sent, "sp", axis=0, tiled=True)
        shares = lax.all_gather(share, ("sp", "tp"), axis=0, tiled=True)
    own_share = jnp.sum(
        jnp.where(expert_ids[None, :] == lax.axis_index("sp"), shares, 0.0), axis=1, keepdims=True
    )
    all_latent = everyone[:, :latent_width]
    all_rot = everyone[:, latent_width:wide]
    keys = jnp.dot(all_latent, plain_key_matrix, preferred_element_type=jnp.float32).astype(
        jnp.bfloat16
    )
    values = jnp.dot(all_latent, value_matrix, preferred_element_type=jnp.float32).astype(
        jnp.bfloat16
    )
    query_rot = turn(
        query_turn.astype(jnp.float32).reshape(tok_dev, heads_dev, QK_ROPE), grid_row, grid_col
    ).astype(jnp.bfloat16)
    scale = (PLAIN_HEAD_WIDTH + QK_ROPE) ** (-0.5)
    attended = []
    for head in range(heads_dev):
        span = slice(head * PLAIN_HEAD_WIDTH, (head + 1) * PLAIN_HEAD_WIDTH)
        scores = (
            jnp.einsum(
                "qd,kd->qk", query_plain[:, span], keys[:, span], preferred_element_type=jnp.float32
            )
            + jnp.einsum(
                "qd,kd->qk", query_rot[:, head], all_rot, preferred_element_type=jnp.float32
            )
        ) * scale
        weights = jnp.exp(scores - jnp.max(scores, axis=1, keepdims=True))
        summed = jnp.dot(
            weights.astype(jnp.bfloat16),
            values[:, head * VALUE_WIDTH : (head + 1) * VALUE_WIDTH],
            preferred_element_type=jnp.float32,
        )
        attended.append(
            (summed / jnp.sum(weights, axis=1, keepdims=True)).astype(jnp.bfloat16)
        )
    attended = jnp.concatenate(attended, axis=1)
    if fits:
        return run_experts(
            attended,
            residual,
            ffn_gain,
            own_share,
            out_weight,
            gate_weight[0],
            up_weight[0],
            down_weight[0],
        )
    swapped = lax.all_to_all(
        attended.reshape(group, rows_dev, heads_dev * VALUE_WIDTH),
        "tp",
        split_axis=0,
        concat_axis=0,
        tiled=True,
    )
    own_rows = jnp.transpose(swapped, (1, 0, 2)).reshape(rows_dev, group * heads_dev * VALUE_WIDTH)
    projected = jnp.dot(own_rows, out_weight, preferred_element_type=jnp.float32)
    hidden = (residual.astype(jnp.float32) + projected).astype(jnp.bfloat16)
    normed = norm_scale(hidden, ffn_gain).astype(jnp.bfloat16)
    rows = lax.all_gather(normed, ("sp", "tp"), axis=0, tiled=True)
    active = expert_active(rows, gate_weight[0], up_weight[0])
    product = jnp.dot(active, down_weight[0], preferred_element_type=jnp.float32)
    mixture = lax.psum_scatter(
        (own_share * product).astype(jnp.bfloat16),
        ("sp", "tp"),
        scatter_dimension=0,
        tiled=True,
    )
    return (hidden.astype(jnp.float32) + mixture.astype(jnp.float32)).astype(jnp.bfloat16)


def solution(mesh):
    placed = (
        P(("grp", "sp"), "tp"),
        P(("grp", "sp"), "tp"),
        P(("grp", "sp"), None),
        P(("grp", "sp"), None),
        P(),
        P(None, "tp"),
        P(None, "tp"),
        P(("grp", "sp", "tp"), None),
        P(),
        P(),
        P("sp", None, "tp"),
        P("sp", None, "tp"),
        P("sp", "tp", None),
        P(("grp", "sp", "tp"), None),
        P(("grp", "sp", "tp"), None),
    )
    return jax.shard_map(
        on_device,
        mesh=mesh,
        in_specs=placed,
        out_specs=P(("grp", "sp", "tp"), None),
        check_vma=False,
    )
```

profile of v0, /device:TPU:8, one launch (start us, length us, event | category | flops | bytes accessed | tf_op | source)
XLA Modules:
  0.0 126.9 jit_solution(18142147822831423362)
XLA Ops:
  0.0 0.0 copy-start
  0.0 0.1 dynamic-slice_convert_fusion
  0.1 0.9 constant_dynamic-slice_fusion
  1.0 0.1 copy.37
  1.1 0.4 fusion.52
  1.5 1.0 fusion.38
  2.5 0.7 convert_element_type.79
  3.2 1.0 fusion.40
  4.2 0.7 select_reduce_fusion.1
  4.9 0.1 copy.33
  5.0 0.1 copy.32
  5.1 0.1 copy.34
  5.2 0.1 concatenate.13.own
  5.4 18.5 %shard_map.145 = bf16[16,80,640]{2,1,0:T(8,128)(2,1)S(1)} custom-call(bf16[80,640]{1,0:T(8,128)(2,1)S(1)} %concatenate.13.own), custom_call_target="tpu_custom_call" | custom-call | tf_op jit(solution)/shard_map/pallas_call | solution.py:203
  23.9 0.0 copy-done
  23.9 0.0 copy-start.3
  23.9 0.8 convolution_convert_fusion.1
  24.7 0.0 copy-start.1
  24.7 1.1 copy-done.1
  25.8 0.0 copy-done.3
  25.8 0.0 copy-start.4
  25.8 0.3 convolution_bitcast_fusion.3
  26.1 0.2 multiply_cosine_fusion.3
  26.3 0.4 copy-done.4
  26.7 0.1 copy.35
  26.9 0.0 copy-start.6
  26.9 0.4 fusion.68
  27.3 0.3 fusion.10
  27.6 0.4 copy-done.6
  27.9 0.0 copy-start.2
  27.9 0.8 convolution_convert_fusion
  28.8 0.3 fusion.6
  29.1 0.1 copy-done.2
  29.3 0.3 convolution_bitcast_fusion.2
  29.5 0.4 fusion.67
  29.9 0.3 fusion.12
  30.2 0.3 fusion.7
  30.6 0.3 convolution_bitcast_fusion.1
  30.8 0.4 fusion.66
  31.2 0.3 fusion.14
  31.5 0.3 fusion.8
  31.9 0.3 convolution_bitcast_fusion
  32.1 0.4 fusion.65
  32.5 0.3 fusion.16
  32.8 0.0 copy-start.5
  32.8 0.3 fusion.9
  33.2 0.7 pad_maximum_fusion
  33.8 0.4 select_reduce_fusion
  34.3 1.3 %reshape_broadcast_in_dim.4.share_ref = f32[16,80,1]{2,1,0:T(8,128)} reshape(f32[1280]{0:T(1024)S(1)} %select_reduce_fusion) | data formatting | bytes 10240 | tf_op jit(solution)/shard_map/reshape;broadcast_in_dim | solution.py:443
  35.6 0.0 copy-done.5
  35.6 0.6 reshape.185.gain_ref
  36.2 89.0 %shard_map.146 = bf16[80,2048]{1,0:T(8,128)(2,1)} custom-call(bf16[2,80,512]{2,1,0:T(8,128)(2,1)} %bitcast.47, bf16[80,2048]{1,0:T(8,128)(2,1)} %residual_ref.1, bf16[1,2048]{1,0:T(2,128)(2,1)} %reshape.185.gain_ref, f32[16,80,1]{2,1,0:T(8,128)} %reshape_broadcast_in_dim.4.share_ref, bf16[1024,2048]{1,0:T(8,128)(2,1)} %out_hbm.1, ...), custom_call_target="tpu_custom_call" | custom-call | tf_op jit(solution)/shard_map/pallas_call | solution.py:406
  125.2 1.7 %copy.39 = bf16[80,2048]{1,0:T(8,128)(2,1)} copy(bf16[80,2048]{1,0:T(8,128)(2,1)} %shard_map.146) | data formatting | bytes 655360
  (13 shorter events, 0.2 us)
Async XLA Ops:
  0.0 23.9 %copy-start = (bf16[512,512]{1,0:T(8,128)(2,1)S(1)}, bf16[512,512]{1,0:T(8,128)(2,1)}, u32[]{:S(2)}) copy-start(bf16[512,512]{1,0:T(8,128)(2,1)} %param.20) | copy-start | bytes 1572868
  23.9 1.9 %copy-start.3 = (bf16[160,512]{1,0:T(8,128)(2,1)S(1)}, bf16[160,512]{1,0:T(8,128)(2,1)}, u32[]{:S(2)}) copy-start(bf16[160,512]{1,0:T(8,128)(2,1)} %param.15) | copy-start | bytes 491524
  24.7 1.1 copy-start.1
  25.8 0.9 copy-start.4
  26.9 1.0 copy-start.6
  27.9 1.3 %copy-start.2 = (bf16[1280,512]{1,0:T(8,128)(2,1)S(1)}, bf16[1280,512]{1,0:T(8,128)(2,1)}, u32[]{:S(2)}) copy-start(bf16[1280,512]{1,0:T(8,128)(2,1)} %copy-done.1) | copy-start | bytes 3932164
  32.8 2.8 %copy-start.5 = (bf16[2048]{0:T(1024)(128)(2,1)S(1)}, bf16[2048]{0:T(1024)(128)(2,1)}, u32[]{:S(2)}) copy-start(bf16[2048]{0:T(1024)(128)(2,1)} %param.24) | copy-start | bytes 12292
where the time goes:
time: 127 us
  Pallas kernels  107 us (84%)
  local copies, waits for them, and re-layouts  7.07 us (6%)
  other arithmetic  6.42 us (5%)
  matrix products  5.72 us (5%)
    pallas_call x1, Pallas kernels, run_experts(): pl.pallas_call(functools.partial(experts_kernel, chips, group), out_shape...  89 us
    pallas_call x1, Pallas kernels, run_gather(): pl.pallas_call(functools.partial(gather_kernel, chips, group), out_shape=...  18.5 us
    unnamed x17, local copies, waits for them, and re-layouts  3.87 us

commit v1 on v0

--- a/solution.py
+++ b/solution.py
@@ -18,7 +18,7 @@
 limit = 7.0
 slope = 1.702
 CORES = 2
-STRIPS = 2
+EARLY_ROWS = 16
 VMEM_BYTES = 60 * 2**20
 
 
@@ -212,9 +212,23 @@
     )(rows)
 
 
+def neighbour_order(chips):
+    table = []
+    for z in range(chips):
+        table.append(sorted(range(chips), key=lambda o: (abs(o - z), o if z < chips // 2 else -o)))
+    return table
+
+
+def pick(z, values):
+    out = values[0]
+    for at in range(1, len(values)):
+        out = jnp.where(z == at, values[at], out)
+    return out
+
+
 def experts_kernel(
     chips,
-    group,
+    early,
     attended_ref,
     residual_ref,
     gain_ref,
@@ -226,13 +240,13 @@
     out_ref,
     heads,
     hidden,
-    rows_ref,
-    total_ref,
     gathered,
     partial,
     from_core,
-    from_tp,
-    from_chip,
+    from_x,
+    from_x_early,
+    from_z,
+    from_z_early,
     outw_ref,
     gate_ref,
     up_ref,
@@ -240,28 +254,57 @@
     load_sem,
     h_send,
     h_recv,
+    gz_send,
+    gz_recv,
+    gx_send,
+    gx_recv,
+    gc_send,
+    gc_recv,
     rc_send,
     rc_recv,
     rx_send,
     rx_recv,
     rz_send,
     rz_recv,
-    *sems,
 ):
+    place = lax.axis_index("sp")
     column = lax.axis_index("tp")
-    core = lax.axis_index("sp") % CORES
-    rows_dev, model_width = rows_ref.shape
-    per_chip = CORES * group
+    chip, core = place // CORES, place % CORES
+    across = 1 - column
+    rows_dev, model_width = hidden.shape
+    late = rows_dev - early
+    table = neighbour_order(chips)
+    order = [chip] + [pick(chip, [table[z][j] for z in range(chips)]) for j in range(1, chips)]
+    far = [0] + [
+        pick(chip, [abs(table[z][j] - z) for z in range(chips)]) for j in range(1, chips)
+    ]
     sends = []
-
-    def launch(copy):
-        copy.start()
-        sends.append(copy)
-
-    greet, met, begin, step, slot, chip_peer, partner, other, remote = gatherer(
-        chips, group, rows_ref, gathered, sems, launch
-    )
-    greet()
+    first_rows = pl.ds(0, early)
+    last_rows = pl.ds(early, late)
+
+    def launch(copy, when=None):
+        if when is None:
+            copy.start()
+        else:
+            pl.when(when)(copy.start)
+        sends.append((copy, when))
+
+    def remote(src, dst, send_sem, recv_sem, device):
+        return pltpu.make_async_remote_copy(
+            src_ref=src, dst_ref=dst, send_sem=send_sem, recv_sem=recv_sem, device_id=device
+        )
+
+    def on_chip(at):
+        return {"sp": at * CORES + core}
+
+    partner = {"sp": chip * CORES + 1 - core}
+    beside = {"tp": across}
+
+    barrier = pltpu.get_barrier_semaphore()
+    pl.semaphore_signal(barrier, inc=1, device_id=partner)
+    pl.semaphore_signal(barrier, inc=1, device_id=beside)
+    for j in range(1, chips):
+        pl.semaphore_signal(barrier, inc=1, device_id=on_chip((chip + j) % chips))
     loads = [
         pltpu.make_async_copy(src, dst, load_sem.at[i])
         for i, (src, dst) in enumerate(
@@ -275,164 +318,321 @@
     ]
     for load in loads:
         load.start()
-    met()
-
-    def heads_copy(shift):
-        return remote(
-            attended_ref.at[other(shift)],
-            heads.at[column],
-            h_send.at[shift],
-            h_recv.at[shift],
-            {"tp": other(shift)},
-        )
-
-    def heads_wait(shift):
-        landed = heads.at[other(group - shift)]
-        remote(
-            landed, landed, h_send.at[shift], h_recv.at[shift], {"tp": other(shift)}
-        ).wait_recv()
-
-    for shift in range(1, group):
-        launch(heads_copy(shift))
+    pl.semaphore_wait(barrier, chips + 1)
+
+    swap = remote(attended_ref.at[across], heads.at[column], h_send, h_recv, beside)
+    launch(swap)
     heads[column] = attended_ref[column]
     loads[0].wait()
-    for shift in range(1, group):
-        heads_wait(shift)
-    joined = jnp.concatenate([heads[at] for at in range(group)], axis=1)
+    landed = heads.at[across]
+    remote(landed, landed, h_send, h_recv, beside).wait_recv()
+    joined = jnp.concatenate([heads[0], heads[1]], axis=1)
     projected = jnp.dot(joined, outw_ref[...], preferred_element_type=jnp.float32)
     mixed = (residual_ref[...].astype(jnp.float32) + projected).astype(jnp.bfloat16)
-    normed = norm_scale(mixed, gain_ref[...]).astype(jnp.bfloat16)
-    rows_ref[...] = normed
-    gathered[slot(0, core, column)] = normed
+    gathered[place, column] = norm_scale(mixed, gain_ref[...]).astype(jnp.bfloat16)
     hidden[...] = mixed
+
+    kinds = ((0, last_rows), (0, first_rows), (1, first_rows), (1, last_rows))
+    use = [k for k in range(4) if (late if k in (0, 3) else early)]
+
+    def piece(at, core_at, kind):
+        flip, rows = kinds[kind]
+        return gathered.at[at * CORES + core_at, across if flip else column, rows]
+
+    def gz_copy(at, kind, to, lane):
+        ref = piece(at, core, kind)
+        return remote(ref, ref, gz_send.at[at, kind, lane], gz_recv.at[at, kind], on_chip(to))
+
+    def gz_wait(at, kind):
+        ref = piece(at, core, kind)
+        remote(
+            ref, ref, gz_send.at[at, kind, 0], gz_recv.at[at, kind], on_chip(at)
+        ).wait_recv()
+
+    def gx_copy(at, kind):
+        ref = piece(at, core, kind)
+        return remote(ref, ref, gx_send.at[at, kind], gx_recv.at[at, kind], beside)
+
+    def gx_wait(at, kind):
+        ref = piece(at, core, 3 - kind)
+        remote(ref, ref, gx_send.at[at, kind], gx_recv.at[at, kind], beside).wait_recv()
+
+    def gc_copy(at, kind):
+        ref = piece(at, core, kind)
+        return remote(ref, ref, gc_send.at[at, kind], gc_recv.at[at, kind], partner)
+
+    def gc_wait(at, kind):
+        ref = piece(at, 1 - core, kind)
+        remote(ref, ref, gc_send.at[at, kind], gc_recv.at[at, kind], partner).wait_recv()
+
+    def both_ways(kind):
+        launch(gz_copy(chip, kind, chip - 1, 0), chip > 0)
+        launch(gz_copy(chip, kind, chip + 1, 1), chip < chips - 1)
+
+    def begin():
+        if early:
+            launch(gx_copy(chip, 1))
+        if late:
+            both_ways(0)
+            launch(gx_copy(chip, 0))
+        if early:
+            both_ways(1)
+        for kind in use:
+            if kind < 2:
+                launch(gc_copy(chip, kind))
+        if early:
+            gx_wait(chip, 1)
+            both_ways(2)
+            launch(gc_copy(chip, 2))
+
+    def forward(at, now=None):
+        step = jnp.where(at < chip, 1, -1)
+        more = jnp.where(at < chip, chip < chips - 1, chip > 0)
+        for kind in use:
+            if kind == 3:
+                continue
+            if now is None:
+                gz_wait(at, kind)
+            else:
+                pl.when(now)(functools.partial(gz_wait, at, kind))
+            launch(gz_copy(at, kind, chip + step, 0), more if now is None else now & more)
+            if kind == 0:
+                launch(gx_copy(at, 0), now)
+            launch(gc_copy(at, kind), now)
+
+    def crossed(at):
+        if late:
+            gx_wait(at, 0)
+            launch(gc_copy(at, 3))
+
+    def apply(load_from, count, store_to):
+        active = expert_active(load_from(gathered).reshape(count, model_width), gate_ref[...], up_ref[...])
+        product = jnp.dot(active, down_ref[...], preferred_element_type=jnp.float32)
+        store_to((product * load_from(share_ref).reshape(count, 1)).astype(jnp.bfloat16))
+
+    def pair(at):
+        return pl.ds(at * CORES, CORES)
+
+    def compute_early(at):
+        if not early:
+            return
+        gc_wait(at, 1)
+        gc_wait(at, 2)
+
+        def store(value):
+            partial[pair(at), :, first_rows] = value.reshape(CORES, 2, early, model_width)
+
+        apply(lambda ref: ref[pair(at), :, first_rows], 2 * CORES * early, store)
+        launch(core_sum_early(at))
+
+    def compute_late(at, kind):
+        if not late:
+            return
+        gc_wait(at, kind)
+        side = across if kind else column
+
+        def store(value):
+            partial[pair(at), side, last_rows] = value.reshape(CORES, late, model_width)
+
+        apply(lambda ref: ref[pair(at), side, last_rows], CORES * late, store)
+        launch(core_sum_late(at, kind))
+
+    def core_sum_early(at):
+        return remote(
+            partial.at[at * CORES + 1 - core, :, first_rows],
+            from_core.at[at, :, first_rows],
+            rc_send.at[at, 1],
+            rc_recv.at[at, 1],
+            partner,
+        )
+
+    def core_sum_late(at, kind):
+        side = across if kind else column
+        return remote(
+            partial.at[at * CORES + 1 - core, side, last_rows],
+            from_core.at[at, side, last_rows],
+            rc_send.at[at, kind],
+            rc_recv.at[at, kind],
+            partner,
+        )
+
+    def x_sum(at):
+        return remote(
+            partial.at[at * CORES + core, across, last_rows],
+            from_x.at[at],
+            rx_send.at[at],
+            rx_recv.at[at],
+            beside,
+        )
+
+    def z_sum_early(at, sender):
+        return remote(
+            partial.at[at * CORES + core, :, first_rows],
+            from_z_early.at[sender],
+            rz_send.at[at, 0],
+            rz_recv.at[sender, 0],
+            on_chip(at),
+        )
+
+    def z_sum_late(at, sender):
+        return remote(
+            partial.at[at * CORES + core, column, last_rows],
+            from_z.at[sender],
+            rz_send.at[at, 1],
+            rz_recv.at[sender, 1],
+            on_chip(at),
+        )
+
+    def wide(value):
+        return value.astype(jnp.float32)
+
+    def sum_early(j):
+        at = order[j]
+        if not early:
+            return
+        core_sum_early(at).wait_recv()
+        mine = at * CORES + core
+        partial[mine, :, first_rows] = (
+            wide(partial[mine, :, first_rows]) + wide(from_core[at, :, first_rows])
+        ).astype(jnp.bfloat16)
+        if j:
+            launch(z_sum_early(at, chip))
+
+    def sum_late(j, kind):
+        at = order[j]
+        if not late:
+            return
+        core_sum_late(at, kind).wait_recv()
+        mine = at * CORES + core
+        side = across if kind else column
+        partial[mine, side, last_rows] = (
+            wide(partial[mine, side, last_rows]) + wide(from_core[at, side, last_rows])
+        ).astype(jnp.bfloat16)
+        if kind:
+            launch(x_sum(at))
+
+    def sum_across(j):
+        at = order[j]
+        if not late:
+            return
+        x_sum(at).wait_recv()
+        mine = at * CORES + core
+        partial[mine, column, last_rows] = (
+            wide(partial[mine, column, last_rows]) + wide(from_x[at])
+        ).astype(jnp.bfloat16)
+        if j:
+            launch(z_sum_late(at, chip))
+
+    def arrive(distance):
+        for j in range(distance, min(2 * distance, chips - 1) + 1):
+            if all(abs(table[z][j] - z) == distance for z in range(chips)):
+                forward(order[j])
+            else:
+                forward(order[j], far[j] == distance)
+
     begin()
-
-    def compute(k):
-        first = slot(k, 0, 0)
-        rows = gathered[pl.ds(first, per_chip)].reshape(per_chip * rows_dev, model_width)
-        active = expert_active(rows, gate_ref[...], up_ref[...])
-        share = share_ref[pl.ds(first, per_chip)].reshape(per_chip * rows_dev, 1)
-        product = jnp.dot(active, down_ref[...], preferred_element_type=jnp.float32)
-        partial[pl.ds(first, per_chip)] = (
-            (product * share).astype(jnp.bfloat16).reshape(per_chip, rows_dev, model_width)
-        )
-
-    def partner_copy(k):
-        return remote(
-            partial.at[pl.ds(slot(k, 1 - core, 0), group)],
-            from_core.at[k],
-            rc_send.at[k],
-            rc_recv.at[k],
-            partner,
-        )
-
-    strips = STRIPS if model_width % (128 * STRIPS) == 0 else 1
-    strip = model_width // strips
-
-    def part(at):
-        return pl.ds(at * strip, strip)
-
-    def tp_sum_copy(k, shift, at):
-        return remote(
-            partial.at[slot(k, core, other(shift)), :, part(at)],
-            from_tp.at[k, shift - 1, :, part(at)],
-            rx_send.at[k, shift, at],
-            rx_recv.at[k, shift, at],
-            {"tp": other(shift)},
-        )
-
-    def chip_sum_copy(k, at):
-        return remote(
-            partial.at[slot(k, core, column), :, part(at)],
-            from_chip.at[k, :, part(at)],
-            rz_send.at[k, at],
-            rz_recv.at[k, at],
-            chip_peer(k),
-        )
-
-    def sum_cores(k):
-        partner_copy(k).wait_recv()
-        first = slot(k, core, 0)
-        partial[pl.ds(first, group)] = (
-            partial[pl.ds(first, group)].astype(jnp.float32) + from_core[k].astype(jnp.float32)
+    for load in loads[1:]:
+        load.wait()
+    compute_early(chip)
+    compute_late(chip, 0)
+    for j in range(chips):
+        at = order[j]
+        if j == 0:
+            arrive(1)
+        crossed(at)
+        if j:
+            compute_early(at)
+            compute_late(at, 0)
+        compute_late(at, 3)
+        sum_early(j)
+        sum_late(j, 3)
+        sum_late(j, 0)
+        if j:
+            sum_across(j - 1)
+            arrive(j + 1)
+    sum_across(chips - 1)
+    mine = chip * CORES + core
+    if early:
+        total = wide(partial[mine, :, first_rows])
+        for j in range(1, chips):
+            z_sum_early(chip, order[j]).wait_recv()
+            total = total + wide(from_z_early[order[j]])
+        partial[mine, :, first_rows] = total.astype(jnp.bfloat16)
+        last = remote(
+            partial.at[mine, across, first_rows],
+            from_x_early,
+            rx_send.at[chips],
+            rx_recv.at[chips],
+            beside,
+        )
+        launch(last)
+    if late:
+        total = wide(hidden[last_rows]) + wide(partial[mine, column, last_rows])
+        for j in range(1, chips):
+            z_sum_late(chip, order[j]).wait_recv()
+            total = total + wide(from_z[order[j]])
+        out_ref[last_rows] = total.astype(jnp.bfloat16)
+    if early:
+        last.wait_recv()
+        out_ref[first_rows] = (
+            wide(hidden[first_rows]) + wide(partial[mine, column, first_rows]) + wide(from_x_early[...])
         ).astype(jnp.bfloat16)
-        for at in range(strips):
-            for shift in range(1, group):
-                launch(tp_sum_copy(k, shift, at))
-
-    def sum_tp(k):
-        for at in range(strips):
-            total = partial[slot(k, core, column), :, part(at)].astype(jnp.float32)
-            for shift in range(1, group):
-                tp_sum_copy(k, shift, at).wait_recv()
-                total = total + from_tp[k, shift - 1, :, part(at)].astype(jnp.float32)
-            if k == 0:
-                total_ref[:, part(at)] = hidden[:, part(at)].astype(jnp.float32) + total
-            else:
-                partial[slot(k, core, column), :, part(at)] = total.astype(jnp.bfloat16)
-                launch(chip_sum_copy(k, at))
-
-    for k in range(chips + 2):
-        if k < chips:
-            step(k)
-            if k == 0:
-                for load in loads[1:]:
-                    load.wait()
-            compute(k)
-            launch(partner_copy(k))
-        if 0 <= k - 1 < chips:
-            sum_cores(k - 1)
-        if 0 <= k - 2 < chips:
-            sum_tp(k - 2)
-    total = total_ref[...]
-    for k in range(1, chips):
-        for at in range(strips):
-            chip_sum_copy(k, at).wait_recv()
-        total = total + from_chip[k].astype(jnp.float32)
-    out_ref[...] = total.astype(jnp.bfloat16)
-    for copy in sends:
-        copy.wait_send()
+    for copy, when in sends:
+        if when is None:
+            copy.wait_send()
+        else:
+            pl.when(when)(copy.wait_send)
 
 
 def run_experts(attended, residual, gain, shares, out_w, gate_w, up_w, down_w):
-    group = lax.axis_size("tp")
     chips = lax.axis_size("sp") // CORES
     rows_dev, model_width = residual.shape
-    blocks = chips * CORES * group
+    pairs = chips * CORES
+    early = EARLY_ROWS if rows_dev > EARLY_ROWS else 0
+    late = rows_dev - early
     dma = pltpu.SemaphoreType.DMA
     block = (rows_dev, model_width)
-    heads = (group, rows_dev, attended.shape[1])
+    heads = (2, rows_dev, attended.shape[1])
     whole = pl.BlockSpec(memory_space=pltpu.VMEM)
+
+    def vmem(*shape):
+        return pltpu.VMEM(shape, jnp.bfloat16)
+
     return pl.pallas_call(
-        functools.partial(experts_kernel, chips, group),
+        functools.partial(experts_kernel, chips, early),
         out_shape=jax.ShapeDtypeStruct(block, jnp.bfloat16),
         in_specs=[whole] * 4 + [pl.BlockSpec(memory_space=pl.ANY)] * 4,
         out_specs=whole,
         scratch_shapes=[
-            pltpu.VMEM(heads, jnp.bfloat16),
-            pltpu.VMEM(block, jnp.bfloat16),
-            pltpu.VMEM(block, jnp.bfloat16),
-            pltpu.VMEM(block, jnp.float32),
-            pltpu.VMEM((blocks,) + block, jnp.bfloat16),
-            pltpu.VMEM((blocks,) + block, jnp.bfloat16),
-            pltpu.VMEM((chips, group) + block, jnp.bfloat16),
-            pltpu.VMEM((chips, group - 1) + block, jnp.bfloat16),
-            pltpu.VMEM((chips,) + block, jnp.bfloat16),
-            pltpu.VMEM(out_w.shape, jnp.bfloat16),
-            pltpu.VMEM(gate_w.shape, jnp.bfloat16),
-            pltpu.VMEM(up_w.shape, jnp.bfloat16),
-            pltpu.VMEM(down_w.shape, jnp.bfloat16),
+            vmem(*heads),
+            vmem(*block),
+            vmem(pairs, 2, *block),
+            vmem(pairs, 2, *block),
+            vmem(chips, 2, *block),
+            vmem(chips, late, model_width),
+            vmem(max(early, 16), model_width),
+            vmem(chips, late, model_width),
+            vmem(chips, 2, max(early, 16), model_width),
+            vmem(*out_w.shape),
+            vmem(*gate_w.shape),
+            vmem(*up_w.shape),
+            vmem(*down_w.shape),
             dma((4,)),
-            dma((group,)),
-            dma((group,)),
-            dma((chips,)),
-            dma((chips,)),
-            dma((chips, group, STRIPS)),
-            dma((chips, group, STRIPS)),
-            dma((chips, STRIPS)),
-            dma((chips, STRIPS)),
-        ]
-        + gather_sems(chips, group),
+            dma,
+            dma,
+            dma((chips, 3, 2)),
+            dma((chips, 3)),
+            dma((chips, 2)),
+            dma((chips, 2)),
+            dma((chips, 4)),
+            dma((chips, 4)),
+            dma((chips, 4)),
+            dma((chips, 4)),
+            dma((chips + 1,)),
+            dma((chips + 1,)),
+            dma((chips, 2)),
+            dma((chips, 2)),
+        ],
         compiler_params=pltpu.CompilerParams(
             collective_id=0, has_side_effects=True, vmem_limit_bytes=VMEM_BYTES
         ),
@@ -440,7 +640,7 @@
         attended.reshape(heads),
         residual,
         gain.reshape(1, model_width),
-        shares.reshape(blocks, rows_dev, 1),
+        shares.reshape(pairs, 2, rows_dev, 1),
         out_w,
         gate_w,
         up_w,
@@ -451,7 +651,7 @@
 def experts_fit(rows_dev, model_width):
     group, places = lax.axis_size("tp"), lax.axis_size("sp")
     chips = places // CORES
-    if group < 2 or places % CORES or chips & (chips - 1) or rows_dev % 16:
+    if group != 2 or places % CORES or chips & (chips - 1) or rows_dev % 16:
         return False
     return 3 * places * group * rows_dev * model_width * 2 < VMEM_BYTES // 2
 

time: 127 us -> 124 us (0.976)
  the two profiles are of different devices: /device:TPU:8 before, /device:TPU:0 now
where the time goes in v1:
time: 124 us; the launch traced here: 123 us
  Pallas kernels  104 us (84%)
  local copies, waits for them, and re-layouts  7.07 us (6%)
  other arithmetic  6.42 us (5%)
  matrix products  5.72 us (5%)
    pallas_call x1, Pallas kernels, run_experts(): pl.pallas_call(functools.partial(experts_kernel, chips, early), out_shape...  82.7 us
    pallas_call x1, Pallas kernels, run_gather(): pl.pallas_call(functools.partial(gather_kernel, chips, group), out_shape=...  21.1 us
    unnamed x17, local copies, waits for them, and re-layouts  3.87 us

profile of v1, /device:TPU:0, one launch (start us, length us, event | category | flops | bytes accessed | tf_op | source)
XLA Modules:
  0.0 123.2 jit_solution(11020857488138668934)
XLA Ops:
  0.0 0.0 copy-start
  0.0 0.1 dynamic-slice_convert_fusion
  0.1 0.9 constant_dynamic-slice_fusion
  1.0 0.1 copy.37
  1.1 0.4 fusion.52
  1.5 1.0 fusion.38
  2.5 0.7 convert_element_type.79
  3.2 1.0 fusion.40
  4.2 0.7 select_reduce_fusion.1
  4.9 0.1 copy.33
  5.0 0.1 copy.32
  5.1 0.1 copy.34
  5.2 0.1 concatenate.13.own
  5.4 21.1 %shard_map.145 = bf16[16,80,640]{2,1,0:T(8,128)(2,1)S(1)} custom-call(bf16[80,640]{1,0:T(8,128)(2,1)S(1)} %concatenate.13.own), custom_call_target="tpu_custom_call" | custom-call | tf_op jit(solution)/shard_map/pallas_call | solution.py:203
  26.5 0.0 copy-done
  26.5 0.0 copy-start.3
  26.5 0.8 convolution_convert_fusion.1
  27.3 0.0 copy-start.1
  27.3 1.1 copy-done.1
  28.4 0.0 copy-done.3
  28.4 0.0 copy-start.4
  28.4 0.3 convolution_bitcast_fusion.3
  28.7 0.2 multiply_cosine_fusion.3
  28.9 0.4 copy-done.4
  29.3 0.1 copy.35
  29.5 0.0 copy-start.6
  29.5 0.4 fusion.68
  29.9 0.3 fusion.10
  30.2 0.3 copy-done.6
  30.5 0.0 copy-start.2
  30.5 0.8 convolution_convert_fusion
  31.4 0.3 fusion.6
  31.7 0.1 copy-done.2
  31.9 0.3 convolution_bitcast_fusion.2
  32.1 0.4 fusion.67
  32.5 0.3 fusion.12
  32.8 0.3 fusion.7
  33.1 0.3 convolution_bitcast_fusion.1
  33.4 0.4 fusion.66
  33.8 0.3 fusion.14
  34.1 0.3 fusion.8
  34.4 0.3 convolution_bitcast_fusion
  34.7 0.4 fusion.65
  35.1 0.3 fusion.16
  35.4 0.0 copy-start.5
  35.4 0.3 fusion.9
  35.7 0.7 pad_maximum_fusion
  36.4 0.4 select_reduce_fusion
  36.9 1.3 %reshape_broadcast_in_dim.4.share_ref = f32[8,2,80,1]{3,2,1,0:T(8,128)} reshape(f32[1280]{0:T(1024)S(1)} %select_reduce_fusion) | data formatting | bytes 10240 | tf_op jit(solution)/shard_map/reshape;broadcast_in_dim | solution.py:643
  38.2 0.0 copy-done.5
  38.2 0.6 reshape.185.gain_ref
  38.8 82.7 %shard_map.146 = bf16[80,2048]{1,0:T(8,128)(2,1)} custom-call(bf16[2,80,512]{2,1,0:T(8,128)(2,1)} %bitcast.47, bf16[80,2048]{1,0:T(8,128)(2,1)} %residual_ref.1, bf16[1,2048]{1,0:T(2,128)(2,1)} %reshape.185.gain_ref, f32[8,2,80,1]{3,2,1,0:T(8,128)} %reshape_broadcast_in_dim.4.share_ref, bf16[1024,2048]{1,0:T(8,128)(2,1)} %out_hbm.1, ...), custom_call_target="tpu_custom_call" | custom-call | tf_op jit(solution)/shard_map/pallas_call | solution.py:601
  121.5 1.7 %copy.39 = bf16[80,2048]{1,0:T(8,128)(2,1)} copy(bf16[80,2048]{1,0:T(8,128)(2,1)} %shard_map.146) | data formatting | bytes 655360
  (13 shorter events, 0.2 us)
Async XLA Ops:
  0.0 26.5 %copy-start = (bf16[512,512]{1,0:T(8,128)(2,1)S(1)}, bf16[512,512]{1,0:T(8,128)(2,1)}, u32[]{:S(2)}) copy-start(bf16[512,512]{1,0:T(8,128)(2,1)} %param.20) | copy-start | bytes 1572868
  26.5 1.9 %copy-start.3 = (bf16[160,512]{1,0:T(8,128)(2,1)S(1)}, bf16[160,512]{1,0:T(8,128)(2,1)}, u32[]{:S(2)}) copy-start(bf16[160,512]{1,0:T(8,128)(2,1)} %param.15) | copy-start | bytes 491524
  27.3 1.1 copy-start.1
  28.4 0.9 copy-start.4
  29.5 1.0 copy-start.6
  30.5 1.3 %copy-start.2 = (bf16[1280,512]{1,0:T(8,128)(2,1)S(1)}, bf16[1280,512]{1,0:T(8,128)(2,1)}, u32[]{:S(2)}) copy-start(bf16[1280,512]{1,0:T(8,128)(2,1)} %copy-done.1) | copy-start | bytes 3932164
  35.4 2.8 %copy-start.5 = (bf16[2048]{0:T(1024)(128)(2,1)S(1)}, bf16[2048]{0:T(1024)(128)(2,1)}, u32[]{:S(2)}) copy-start(bf16[2048]{0:T(1024)(128)(2,1)} %param.24) | copy-start | bytes 12292

commit v2 on v1

--- a/solution.py
+++ b/solution.py
@@ -2,6 +2,7 @@
 
 import jax
 import jax.numpy as jnp
+import numpy as np
 from jax import lax
 from jax.experimental import pallas as pl
 from jax.experimental.pallas import tpu as pltpu
@@ -18,7 +19,7 @@
 limit = 7.0
 slope = 1.702
 CORES = 2
-EARLY_ROWS = 16
+EARLY_ROWS = 32
 VMEM_BYTES = 60 * 2**20
 
 
@@ -173,7 +174,53 @@
     return greet, met, begin, step, slot, chip_peer, partner, other, remote
 
 
-def gather_kernel(chips, group, own, gathered, *sems):
+def turn_matrices(shape, width):
+    row = lax.broadcasted_iota(jnp.int32, shape, 0)
+    col = lax.broadcasted_iota(jnp.int32, shape, 1)
+    count = width // 4
+    lane = col % 128
+    source = (col // 128) * width + lane
+    inside = lane < width
+    lower = lane % (2 * count) < count
+    straight = jnp.where(inside & (row == source), 1.0, 0.0)
+    moved = jnp.where(lower, source + count, source - count)
+    sign = jnp.where(lower, -1.0, 1.0)
+    crossed = jnp.where(inside & (row == moved), sign, 0.0)
+    return straight.astype(jnp.bfloat16), crossed.astype(jnp.bfloat16)
+
+
+def attention_kernel(
+    chips,
+    group,
+    query_ref,
+    query_turn_ref,
+    latent_ref,
+    key_turn_ref,
+    gain_ref,
+    freqs_ref,
+    routes_ref,
+    route_weights_ref,
+    keyw_hbm,
+    valuew_hbm,
+    out_ref,
+    share_ref,
+    own,
+    gathered,
+    queries,
+    cosines,
+    sines,
+    keyw_ref,
+    valuew_ref,
+    load_sem,
+    *sems,
+):
+    place = lax.axis_index("sp")
+    column = lax.axis_index("tp")
+    tokens, latent_width = latent_ref.shape
+    rows_dev = own.shape[0]
+    heads_dev = query_ref.shape[1] // PLAIN_HEAD_WIDTH
+    count = lax.axis_size("sp")
+    per_chip = CORES * group
     sends = []
 
     def launch(copy):
@@ -182,11 +229,107 @@
 
     greet, met, begin, step, slot = gatherer(chips, group, own, gathered, sems, launch)[:5]
     greet()
+    loads = [
+        pltpu.make_async_copy(keyw_hbm, keyw_ref, load_sem.at[0]),
+        pltpu.make_async_copy(valuew_hbm, valuew_ref, load_sem.at[1]),
+    ]
+    for load in loads:
+        load.start()
+
+    at = place * tokens + lax.broadcasted_iota(jnp.int32, (tokens, 128), 0)
+    lane = lax.broadcasted_iota(jnp.int32, (tokens, 128), 1)
+    shift = jnp.where(lane < QK_ROPE // 2, at // GRID_W, at % GRID_W).astype(jnp.float32)
+    angle = shift * freqs_ref[...]
+    cosines[...] = jnp.cos(angle)
+    sines[...] = jnp.sin(angle)
+
+    def turned(vector, matrices, cos, sin):
+        straight, crossed = (
+            jnp.dot(vector, matrix, preferred_element_type=jnp.float32) for matrix in matrices
+        )
+        return straight * cos + crossed * sin
+
+    mine = pl.ds(pl.multiple_of(column * rows_dev, 16), rows_dev)
+    key_rot = turned(
+        key_turn_ref[mine, :],
+        turn_matrices((QK_ROPE, 128), QK_ROPE),
+        cosines[mine, :],
+        sines[mine, :],
+    )
+    lane = lax.broadcasted_iota(jnp.int32, (rows_dev, 128), 1) - QK_ROPE
+    expert = jnp.where(lane < count, lane, lane - count)
+    share = jnp.zeros((rows_dev, 128), jnp.float32)
+    for k in range(routes_ref.shape[1]):
+        share = share + jnp.where(
+            routes_ref[:, k : k + 1] == expert, route_weights_ref[:, k : k + 1], 0.0
+        )
+    high = share.astype(jnp.bfloat16).astype(jnp.float32)
+    packed = jnp.where(lane < count, high, share - high)
+    packed = jnp.where(lane < 2 * count, packed, 0.0)
+    own[:, :latent_width] = norm_scale(latent_ref[mine, :], gain_ref[...]).astype(jnp.bfloat16)
+    own[:, latent_width:] = jnp.where(lane < 0, key_rot, packed).astype(jnp.bfloat16)
     met()
     begin()
-    gathered[slot(0, lax.axis_index("sp") % CORES, lax.axis_index("tp"))] = own[...]
+    gathered[slot(0, place % CORES, column)] = own[...]
+
+    matrices = turn_matrices((heads_dev * QK_ROPE, heads_dev * 128), QK_ROPE)
+    straight, crossed = (
+        jnp.dot(query_turn_ref[...], matrix, preferred_element_type=jnp.float32)
+        for matrix in matrices
+    )
+    for head in range(heads_dev):
+        span = slice(head * 128, (head + 1) * 128)
+        queries[head, :, :128] = query_ref[:, span]
+        queries[head, :, 128:] = (
+            straight[:, span] * cosines[...] + crossed[:, span] * sines[...]
+        ).astype(jnp.bfloat16)
+    for load in loads:
+        load.wait()
+
+    scale = (PLAIN_HEAD_WIDTH + QK_ROPE) ** (-0.5)
+    peaks = [None] * heads_dev
+    sums = [None] * heads_dev
+    totals = [None] * heads_dev
     for k in range(chips):
         step(k)
+        first = slot(k, 0, 0)
+        width = per_chip * rows_dev
+        latents = gathered[pl.ds(first, per_chip), :, :latent_width].reshape(width, latent_width)
+        rot = gathered[pl.ds(first, per_chip), :, latent_width:].reshape(width, 128)
+        keys = jnp.dot(latents, keyw_ref[...], preferred_element_type=jnp.float32).astype(
+            jnp.bfloat16
+        )
+        values = jnp.dot(latents, valuew_ref[...], preferred_element_type=jnp.float32).astype(
+            jnp.bfloat16
+        )
+        for head in range(heads_dev):
+            span = slice(head * 128, (head + 1) * 128)
+            scores = scale * lax.dot_general(
+                queries[head],
+                jnp.concatenate([keys[:, span], rot], axis=1),
+                (((1,), (1,)), ((), ())),
+                preferred_element_type=jnp.float32,
+            )
+            peak = jnp.max(scores, axis=1, keepdims=True)
+            if k:
+                peak = jnp.maximum(peak, peaks[head])
+            weights = jnp.exp(scores - peak)
+            total = jnp.sum(weights, axis=1, keepdims=True)
+            summed = jnp.dot(
+                weights.astype(jnp.bfloat16), values[:, span], preferred_element_type=jnp.float32
+            )
+            if k:
+                fade = jnp.exp(peaks[head] - peak)
+                total = total + fade * sums[head]
+                summed = summed + fade * totals[head]
+            peaks[head], sums[head], totals[head] = peak, total, summed
+        lane = lax.broadcasted_iota(jnp.int32, (width, 128), 1) - QK_ROPE
+        named = (lane == place) | (lane == place + count)
+        share_ref[pl.ds(first, per_chip)] = jnp.sum(
+            jnp.where(named, rot.astype(jnp.float32), 0.0), axis=1, keepdims=True
+        ).reshape(per_chip, rows_dev, 1)
+    for head in range(heads_dev):
+        out_ref[:, head * 128 : (head + 1) * 128] = (totals[head] / sums[head]).astype(jnp.bfloat16)
     for copy in sends:
         copy.wait_send()
 
@@ -196,20 +339,53 @@
     return [dma((chips,))] * 2 + [dma((chips, group))] * 4
 
 
-def run_gather(rows):
+def run_attention(query, query_turn, latent, key_turn, gain, routes, route_weights, key_w, value_w):
     group = lax.axis_size("tp")
     chips = lax.axis_size("sp") // CORES
+    blocks = chips * CORES * group
+    tokens, latent_width = latent.shape
+    rows_dev = routes.shape[0]
+    heads_dev = query.shape[1] // PLAIN_HEAD_WIDTH
+    quarter = QK_ROPE // 4
+    freqs = theta ** (-np.arange(quarter, dtype=np.float32) / np.float32(quarter))
+    freqs = np.tile(freqs.astype(np.float32), 128 // quarter).reshape(1, 128)
+    dma = pltpu.SemaphoreType.DMA
     whole = pl.BlockSpec(memory_space=pltpu.VMEM)
+    sent = latent_width + 128
     return pl.pallas_call(
-        functools.partial(gather_kernel, chips, group),
-        out_shape=jax.ShapeDtypeStruct((chips * CORES * group,) + rows.shape, rows.dtype),
-        in_specs=[whole],
-        out_specs=whole,
-        scratch_shapes=gather_sems(chips, group),
+        functools.partial(attention_kernel, chips, group),
+        out_shape=[
+            jax.ShapeDtypeStruct((tokens, heads_dev * VALUE_WIDTH), jnp.bfloat16),
+            jax.ShapeDtypeStruct((blocks, rows_dev, 1), jnp.float32),
+        ],
+        in_specs=[whole] * 8 + [pl.BlockSpec(memory_space=pl.ANY)] * 2,
+        out_specs=[whole, whole],
+        scratch_shapes=[
+            pltpu.VMEM((rows_dev, sent), jnp.bfloat16),
+            pltpu.VMEM((blocks, rows_dev, sent), jnp.bfloat16),
+            pltpu.VMEM((heads_dev, tokens, 256), jnp.bfloat16),
+            pltpu.VMEM((tokens, 128), jnp.float32),
+            pltpu.VMEM((tokens, 128), jnp.float32),
+            pltpu.VMEM(key_w.shape, jnp.bfloat16),
+            pltpu.VMEM(value_w.shape, jnp.bfloat16),
+            dma((2,)),
+        ]
+        + gather_sems(chips, group),
         compiler_params=pltpu.CompilerParams(
             collective_id=1, has_side_effects=True, vmem_limit_bytes=VMEM_BYTES // 2
         ),
-    )(rows)
+    )(
+        query,
+        query_turn,
+        latent,
+        key_turn,
+        gain.reshape(1, latent_width),
+        jnp.asarray(freqs),
+        routes,
+        route_weights,
+        key_w,
+        value_w,
+    )
 
 
 def neighbour_order(chips):
@@ -648,10 +824,12 @@
     )
 
 
-def experts_fit(rows_dev, model_width):
+def experts_fit(tokens, rows_dev, model_width):
     group, places = lax.axis_size("tp"), lax.axis_size("sp")
     chips = places // CORES
     if group != 2 or places % CORES or chips & (chips - 1) or rows_dev % 16:
+        return False
+    if tokens != group * rows_dev or QK_ROPE + 2 * places > 128:
         return False
     return 3 * places * group * rows_dev * model_width * 2 < VMEM_BYTES // 2
 
@@ -673,6 +851,28 @@
     routes,
     route_weights,
 ):
+    if experts_fit(latent.shape[0], *residual.shape):
+        attended, own_share = run_attention(
+            query_plain,
+            query_turn,
+            latent,
+            key_turn,
+            latent_norm_scale,
+            routes,
+            route_weights,
+            plain_key_matrix,
+            value_matrix,
+        )
+        return run_experts(
+            attended,
+            residual,
+            ffn_gain,
+            own_share,
+            out_weight,
+            gate_weight[0],
+            up_weight[0],
+            down_weight[0],
+        )
     tok_dev = latent.shape[0]
     heads_dev = query_plain.shape[1] // PLAIN_HEAD_WIDTH
     model_width = residual.shape[1]
@@ -682,7 +882,6 @@
     rows_dev, model_width = residual.shape
     group = lax.axis_size("tp")
     count = lax.axis_size("sp")
-    fits = experts_fit(rows_dev, model_width)
     expert_ids = jnp.arange(count, dtype=jnp.int32)
     share = jnp.sum(
         route_weights[..., None] * (routes[..., None] == expert_ids).astype(jnp.float32), axis=1
@@ -695,30 +894,9 @@
         key_rot = turn(turns.astype(jnp.float32), at_row, at_col).astype(jnp.bfloat16)
         return [normed_latent, key_rot]
 
-    if fits:
-        first = lax.axis_index("tp") * rows_dev
-        high = lax.reduce_precision(share, 8, 7)
-        filled = wide + 2 * count
-        sent = jnp.concatenate(
-            key_side(
-                lax.dynamic_slice_in_dim(latent, first, rows_dev, 0),
-                lax.dynamic_slice_in_dim(key_turn, first, rows_dev, 0),
-                lax.dynamic_slice_in_dim(grid_row, first, rows_dev, 0),
-                lax.dynamic_slice_in_dim(grid_col, first, rows_dev, 0),
-            )
-            + [high.astype(jnp.bfloat16), (share - high).astype(jnp.bfloat16)]
-            + [jnp.zeros((rows_dev, -filled % 128), jnp.bfloat16)],
-            axis=1,
-        )
-        everyone = run_gather(sent)
-        everyone = everyone.reshape(everyone.shape[0] * rows_dev, everyone.shape[2])
-        shares = everyone[:, wide : wide + count].astype(jnp.float32) + everyone[
-            :, wide + count : filled
-        ].astype(jnp.float32)
-    else:
-        sent = jnp.concatenate(key_side(latent, key_turn, grid_row, grid_col), axis=1)
-        everyone = lax.all_gather(sent, "sp", axis=0, tiled=True)
-        shares = lax.all_gather(share, ("sp", "tp"), axis=0, tiled=True)
+    sent = jnp.concatenate(key_side(latent, key_turn, grid_row, grid_col), axis=1)
+    everyone = lax.all_gather(sent, "sp", axis=0, tiled=True)
+    shares = lax.all_gather(share, ("sp", "tp"), axis=0, tiled=True)
     own_share = jnp.sum(
         jnp.where(expert_ids[None, :] == lax.axis_index("sp"), shares, 0.0), axis=1, keepdims=True
     )
@@ -755,17 +933,6 @@
             (summed / jnp.sum(weights, axis=1, keepdims=True)).astype(jnp.bfloat16)
         )
     attended = jnp.concatenate(attended, axis=1)
-    if fits:
-        return run_experts(
-            attended,
-            residual,
-            ffn_gain,
-            own_share,
-            out_weight,
-            gate_weight[0],
-            up_weight[0],
-            down_weight[0],
-        )
     swapped = lax.all_to_all(
         attended.reshape(group, rows_dev, heads_dev * VALUE_WIDTH),
         "tp",

time: 124 us -> 118 us (0.952)
  other arithmetic: 6.42 us -> 0 us
  local copies, waits for them, and re-layouts: 7.07 us -> 13.1 us
  matrix products: 5.72 us -> 0 us
    unnamed x17 -> x20, local copies, waits for them, and re-layouts: 3.87 us -> 11.1 us
    dot_general x14 -> x0, matrix products: 5.72 us -> none  [the longest x4 1.62 us: on_device(): jnp.einsum('qd,kd->qk', query_rot[:, head], all_rot, preferred_element_ty...]
    reduce_sum x7 -> x0, other arithmetic: 3.24 us -> none  [the longest x4 1.09 us: on_device(): jnp.sum(weights, axis=1, keepdims=True)]
    pallas_call x1, Pallas kernels: 21.1 us -> 23.7 us  [run_attention(): pl.pallas_call(functools.partial(attention_kernel, chips, group), out_sha...]
    pallas_call x1, Pallas kernels: 82.7 us -> 80.2 us  [run_experts(): pl.pallas_call(functools.partial(experts_kernel, chips, early), out_shape...]
    convert_element_type x6 -> x0, other arithmetic: 1.77 us -> none  [the longest x1 0.97 us: key_side(): normed_latent = norm_scale(latents, latent_norm_scale).astype(jnp.bfloat16)]
    another operation x1 -> x0, local copies, waits for them, and re-layouts: 1.31 us -> none  [run_experts(): shares.reshape(pairs, 2, rows_dev, 1)]
where the time goes in v2:
time: 118 us; the launch traced here: 117 us
  Pallas kernels  104 us (88%)
  local copies, waits for them, and re-layouts  13.1 us (11%)
    pallas_call x1, Pallas kernels, run_experts(): pl.pallas_call(functools.partial(experts_kernel, chips, early), out_shape...  80.2 us
    pallas_call x1, Pallas kernels, run_attention(): pl.pallas_call(functools.partial(attention_kernel, chips, group), out_sha...  23.7 us
    unnamed x20, local copies, waits for them, and re-layouts  11.1 us

profile of v2, /device:TPU:0, one launch (start us, length us, event | category | flops | bytes accessed | tf_op | source)
XLA Modules:
  0.0 117.0 jit_solution(12410305313775044985)
XLA Ops:
  0.0 0.7 reshape.12.gain_ref
  0.7 1.3 %reshape.14.gain_ref = bf16[1,2048]{1,0:T(2,128)(2,1)} reshape(bf16[2048]{0:T(1024)(128)(2,1)} %param.25) | data formatting | bytes 8192 | tf_op jit(solution)/shard_map/reshape | solution.py:818
  2.0 0.9 copy.17.key_turn_ref
  2.8 0.8 copy.18.routes_ref
  3.6 0.8 copy.19.route_weights_ref
  4.4 0.0 copy-start.1
  4.4 1.0 copy-done.1
  5.4 0.0 copy-start.2
  5.4 1.0 copy-done.2
  6.5 0.0 copy-start.3
  6.5 0.9 copy-done.3
  7.4 0.0 copy-start.4
  7.4 0.9 copy-done.4
  8.3 0.0 copy-start.6
  8.3 0.9 copy-done.6
  9.2 0.0 copy-start.7
  9.2 0.7 copy-done.7
  9.9 23.7 %shard_map.154 = (bf16[160,512]{1,0:T(8,128)(2,1)S(1)}, f32[16,80,1]{2,1,0:T(8,128)S(1)}) custom-call(bf16[160,512]{1,0:T(8,128)(2,1)S(1)} %copy-done.3, bf16[160,256]{1,0:T(8,128)(2,1)S(1)} %copy-done.6, bf16[160,512]{1,0:T(8,128)(2,1)S(1)} %copy-done.4, bf16[160,64]{1,0:T(8,128)(2,1)S(1)} %copy.17.key_turn_ref, bf16[1,512]{1,0:T(2,128)(2,1)S(1)} %reshape.12.gain_ref, ...), custom_call_target="tpu_custom_call" | custom-call | tf_op jit(solution)/shard_map/pallas_call | solution.py:355
  33.6 0.0 copy-start
  33.6 0.8 copy-done
  34.4 0.0 copy-start.5
  34.4 0.7 copy-done.5
  35.1 80.2 %shard_map.155 = bf16[80,2048]{1,0:T(8,128)(2,1)} custom-call(bf16[2,80,512]{2,1,0:T(8,128)(2,1)} %bitcast.6, bf16[80,2048]{1,0:T(8,128)(2,1)} %residual_ref.1, bf16[1,2048]{1,0:T(2,128)(2,1)} %reshape.14.gain_ref, f32[8,2,80,1]{3,2,1,0:T(8,128)} %bitcast.5, bf16[1024,2048]{1,0:T(8,128)(2,1)} %out_hbm.1, bf16[2048,512]{1,0:T(8,128)(2,1)} %bitcast.7, ...), custom_call_target="tpu_custom_call" | custom-call | tf_op jit(solution)/shard_map/pallas_call | solution.py:777
  115.3 1.7 %copy.21 = bf16[80,2048]{1,0:T(8,128)(2,1)} copy(bf16[80,2048]{1,0:T(8,128)(2,1)} %shard_map.155) | data formatting | bytes 655360
Async XLA Ops:
  4.4 1.0 copy-start.1
  5.4 1.0 copy-start.2
  6.5 0.9 copy-start.3
  7.4 0.9 copy-start.4
  8.3 0.9 copy-start.6
  9.2 0.7 copy-start.7
  33.6 0.8 copy-start
  34.4 0.7 copy-start.5

commit v3 on v2

--- a/solution.py
+++ b/solution.py
@@ -192,33 +192,28 @@
 def attention_kernel(
     chips,
     group,
-    query_ref,
-    query_turn_ref,
-    latent_ref,
-    key_turn_ref,
-    gain_ref,
-    freqs_ref,
-    routes_ref,
-    route_weights_ref,
-    keyw_hbm,
-    valuew_hbm,
-    out_ref,
-    share_ref,
-    own,
-    gathered,
-    queries,
-    cosines,
-    sines,
-    keyw_ref,
-    valuew_ref,
-    load_sem,
-    *sems,
+    *refs,
 ):
+    inputs, refs = refs[:10], refs[10:]
+    out_ref, share_ref, own, gathered, queries, cosines, sines, key_turns = refs[:8]
+    held, load_sem, sems = refs[8:18], refs[18], refs[19:]
+    (
+        latent_ref,
+        gain_ref,
+        freqs_ref,
+        key_turn_ref,
+        routes_ref,
+        route_weights_ref,
+        query_turn_ref,
+        query_ref,
+        keyw_ref,
+        valuew_ref,
+    ) = held
     place = lax.axis_index("sp")
     column = lax.axis_index("tp")
-    tokens, latent_width = latent_ref.shape
+    tokens, latent_width = inputs[0].shape
     rows_dev = own.shape[0]
-    heads_dev = query_ref.shape[1] // PLAIN_HEAD_WIDTH
+    heads_dev = inputs[7].shape[1] // PLAIN_HEAD_WIDTH
     count = lax.axis_size("sp")
     per_chip = CORES * group
     sends = []
@@ -230,11 +225,12 @@
     greet, met, begin, step, slot = gatherer(chips, group, own, gathered, sems, launch)[:5]
     greet()
     loads = [
-        pltpu.make_async_copy(keyw_hbm, keyw_ref, load_sem.at[0]),
-        pltpu.make_async_copy(valuew_hbm, valuew_ref, load_sem.at[1]),
+        pltpu.make_async_copy(src, dst, load_sem.at[i])
+        for i, (src, dst) in enumerate(zip(inputs, held))
     ]
     for load in loads:
         load.start()
+    loads[2].wait()
 
     at = place * tokens + lax.broadcasted_iota(jnp.int32, (tokens, 128), 0)
     lane = lax.broadcasted_iota(jnp.int32, (tokens, 128), 1)
@@ -250,8 +246,13 @@
         return straight * cos + crossed * sin
 
     mine = pl.ds(pl.multiple_of(column * rows_dev, 16), rows_dev)
+    for load in loads[:2] + loads[3:6]:
+        load.wait()
+    key_turns[...] = key_turn_ref[...].T
+    named = routes_ref[...].T
+    weighing = route_weights_ref[...].T
     key_rot = turned(
-        key_turn_ref[mine, :],
+        key_turns[mine, :],
         turn_matrices((QK_ROPE, 128), QK_ROPE),
         cosines[mine, :],
         sines[mine, :],
@@ -259,19 +260,19 @@
     lane = lax.broadcasted_iota(jnp.int32, (rows_dev, 128), 1) - QK_ROPE
     expert = jnp.where(lane < count, lane, lane - count)
     share = jnp.zeros((rows_dev, 128), jnp.float32)
-    for k in range(routes_ref.shape[1]):
-        share = share + jnp.where(
-            routes_ref[:, k : k + 1] == expert, route_weights_ref[:, k : k + 1], 0.0
-        )
+    for k in range(named.shape[1]):
+        share = share + jnp.where(named[:, k : k + 1] == expert, weighing[:, k : k + 1], 0.0)
     high = share.astype(jnp.bfloat16).astype(jnp.float32)
     packed = jnp.where(lane < count, high, share - high)
     packed = jnp.where(lane < 2 * count, packed, 0.0)
-    own[:, :latent_width] = norm_scale(latent_ref[mine, :], gain_ref[...]).astype(jnp.bfloat16)
+    own[:, :latent_width] = norm_scale(latent_ref[mine, :], gain_ref[...].reshape(1, latent_width)).astype(jnp.bfloat16)
     own[:, latent_width:] = jnp.where(lane < 0, key_rot, packed).astype(jnp.bfloat16)
     met()
     begin()
     gathered[slot(0, place % CORES, column)] = own[...]
 
+    for load in loads[6:]:
+        load.wait()
     matrices = turn_matrices((heads_dev * QK_ROPE, heads_dev * 128), QK_ROPE)
     straight, crossed = (
         jnp.dot(query_turn_ref[...], matrix, preferred_element_type=jnp.float32)
@@ -283,8 +284,6 @@
         queries[head, :, 128:] = (
             straight[:, span] * cosines[...] + crossed[:, span] * sines[...]
         ).astype(jnp.bfloat16)
-    for load in loads:
-        load.wait()
 
     scale = (PLAIN_HEAD_WIDTH + QK_ROPE) ** (-0.5)
     peaks = [None] * heads_dev
@@ -352,13 +351,25 @@
     dma = pltpu.SemaphoreType.DMA
     whole = pl.BlockSpec(memory_space=pltpu.VMEM)
     sent = latent_width + 128
+    arrays = (
+        latent,
+        gain,
+        jnp.asarray(freqs),
+        key_turn.T,
+        routes.T,
+        route_weights.T,
+        query_turn,
+        query,
+        key_w,
+        value_w,
+    )
     return pl.pallas_call(
         functools.partial(attention_kernel, chips, group),
         out_shape=[
             jax.ShapeDtypeStruct((tokens, heads_dev * VALUE_WIDTH), jnp.bfloat16),
             jax.ShapeDtypeStruct((blocks, rows_dev, 1), jnp.float32),
         ],
-        in_specs=[whole] * 8 + [pl.BlockSpec(memory_space=pl.ANY)] * 2,
+        in_specs=[pl.BlockSpec(memory_space=pltpu.HBM)] * len(arrays),
         out_specs=[whole, whole],
         scratch_shapes=[
             pltpu.VMEM((rows_dev, sent), jnp.bfloat16),
@@ -366,26 +377,15 @@
             pltpu.VMEM((heads_dev, tokens, 256), jnp.bfloat16),
             pltpu.VMEM((tokens, 128), jnp.float32),
             pltpu.VMEM((tokens, 128), jnp.float32),
-            pltpu.VMEM(key_w.shape, jnp.bfloat16),
-            pltpu.VMEM(value_w.shape, jnp.bfloat16),
-            dma((2,)),
+            pltpu.VMEM((tokens, QK_ROPE), jnp.bfloat16),
         ]
+        + [pltpu.VMEM(array.shape, array.dtype) for array in arrays]
+        + [dma((len(arrays),))]
         + gather_sems(chips, group),
         compiler_params=pltpu.CompilerParams(
-            collective_id=1, has_side_effects=True, vmem_limit_bytes=VMEM_BYTES // 2
+            collective_id=1, has_side_effects=True, vmem_limit_bytes=VMEM_BYTES
         ),
-    )(
-        query,
-        query_turn,
-        latent,
-        key_turn,
-        gain.reshape(1, latent_width),
-        jnp.asarray(freqs),
-        routes,
-        route_weights,
-        key_w,
-        value_w,
-    )
+    )(*arrays)
 
 
 def neighbour_order(chips):
@@ -406,9 +406,9 @@
     chips,
     early,
     attended_ref,
-    residual_ref,
-    gain_ref,
     share_ref,
+    residual_hbm,
+    gain_hbm,
     out_hbm,
     gate_hbm,
     up_hbm,
@@ -423,6 +423,8 @@
     from_x_early,
     from_z,
     from_z_early,
+    residual_ref,
+    gain_ref,
     outw_ref,
     gate_ref,
     up_ref,
@@ -485,6 +487,8 @@
         pltpu.make_async_copy(src, dst, load_sem.at[i])
         for i, (src, dst) in enumerate(
             (
+                (residual_hbm, residual_ref),
+                (gain_hbm, gain_ref),
                 (out_hbm, outw_ref),
                 (gate_hbm, gate_ref),
                 (up_hbm, up_ref),
@@ -499,13 +503,14 @@
     swap = remote(attended_ref.at[across], heads.at[column], h_send, h_recv, beside)
     launch(swap)
     heads[column] = attended_ref[column]
-    loads[0].wait()
+    for load in loads[:3]:
+        load.wait()
     landed = heads.at[across]
     remote(landed, landed, h_send, h_recv, beside).wait_recv()
     joined = jnp.concatenate([heads[0], heads[1]], axis=1)
     projected = jnp.dot(joined, outw_ref[...], preferred_element_type=jnp.float32)
     mixed = (residual_ref[...].astype(jnp.float32) + projected).astype(jnp.bfloat16)
-    gathered[place, column] = norm_scale(mixed, gain_ref[...]).astype(jnp.bfloat16)
+    gathered[place, column] = norm_scale(mixed, gain_ref[...].reshape(1, model_width)).astype(jnp.bfloat16)
     hidden[...] = mixed
 
     kinds = ((0, last_rows), (0, first_rows), (1, first_rows), (1, last_rows))
@@ -707,7 +712,7 @@
                 forward(order[j], far[j] == distance)
 
     begin()
-    for load in loads[1:]:
+    for load in loads[3:]:
         load.wait()
     compute_early(chip)
     compute_late(chip, 0)
@@ -777,7 +782,7 @@
     return pl.pallas_call(
         functools.partial(experts_kernel, chips, early),
         out_shape=jax.ShapeDtypeStruct(block, jnp.bfloat16),
-        in_specs=[whole] * 4 + [pl.BlockSpec(memory_space=pl.ANY)] * 4,
+        in_specs=[whole] * 2 + [pl.BlockSpec(memory_space=pltpu.HBM)] * 6,
         out_specs=whole,
         scratch_shapes=[
             vmem(*heads),
@@ -789,11 +794,13 @@
             vmem(max(early, 16), model_width),
             vmem(chips, late, model_width),
             vmem(chips, 2, max(early, 16), model_width),
+            vmem(*block),
+            vmem(*gain.shape),
             vmem(*out_w.shape),
             vmem(*gate_w.shape),
             vmem(*up_w.shape),
             vmem(*down_w.shape),
-            dma((4,)),
+            dma((6,)),
             dma,
             dma,
             dma((chips, 3, 2)),
@@ -814,9 +821,9 @@
         ),
     )(
         attended.reshape(heads),
+        shares.reshape(pairs, 2, rows_dev, 1),
         residual,
-        gain.reshape(1, model_width),
-        shares.reshape(pairs, 2, rows_dev, 1),
+        gain,
         out_w,
         gate_w,
         up_w,

time: 118 us -> 108 us (0.915)
  local copies, waits for them, and re-layouts: 13.1 us -> 1.72 us
  Pallas kernels: 104 us -> 106 us
    unnamed x20 -> x1, local copies, waits for them, and re-layouts: 11.1 us -> 1.72 us
    reshape x2 -> x0, local copies, waits for them, and re-layouts: 1.97 us -> none  [the longest x1 1.29 us: run_experts(): gain.reshape(1, model_width)]
    pallas_call x1, Pallas kernels: 23.7 us -> 25.2 us  [run_attention(): pl.pallas_call(functools.partial(attention_kernel, chips, group), out_sha...]
where the time goes in v3:
time: 108 us; the launch traced here: 107 us
  Pallas kernels  106 us (98%)
  local copies, waits for them, and re-layouts  1.72 us (2%)
    pallas_call x1, Pallas kernels, run_experts(): pl.pallas_call(functools.partial(experts_kernel, chips, early), out_shape...  80.4 us
    pallas_call x1, Pallas kernels, run_attention(): pl.pallas_call(functools.partial(attention_kernel, chips, group), out_sha...  25.2 us

profile of v3, /device:TPU:0, one launch (start us, length us, event | category | flops | bytes accessed | tf_op | source)
XLA Modules:
  0.0 107.4 jit_solution(2735293837188261469)
XLA Ops:
  0.0 25.2 %shard_map.154 = (bf16[160,512]{1,0:T(8,128)(2,1)}, f32[16,80,1]{2,1,0:T(8,128)}) custom-call(bf16[160,512]{1,0:T(8,128)(2,1)} %refs_0_.1, bf16[512]{0:T(512)(128)(2,1)} %refs_1_.1, f32[1,128]{1,0:T(1,128)} %constant.2.clone.refs_2_, bf16[64,160]{1,0:T(8,128)(2,1)} %bitcast.13, s32[4,80]{1,0:T(4,128)} %bitcast.14, f32[4,80]{1,0:T(4,128)} %bitcast.15, ...), custom_call_target="tpu_custom_call" | custom-call | tf_op jit(solution)/shard_map/pallas_call | solution.py:366
  25.2 80.4 %shard_map.155 = bf16[80,2048]{1,0:T(8,128)(2,1)} custom-call(bf16[2,80,512]{2,1,0:T(8,128)(2,1)} %bitcast.12, f32[8,2,80,1]{3,2,1,0:T(8,128)} %bitcast.11, bf16[80,2048]{1,0:T(8,128)(2,1)} %residual_hbm.1, bf16[2048]{0:T(1024)(128)(2,1)} %gain_hbm.1, bf16[1024,2048]{1,0:T(8,128)(2,1)} %out_hbm.1, bf16[2048,512]{1,0:T(8,128)(2,1)} %bitcast.8, ...), custom_call_target="tpu_custom_call" | custom-call | tf_op jit(solution)/shard_map/pallas_call | solution.py:782
  105.6 1.7 %copy.18 = bf16[80,2048]{1,0:T(8,128)(2,1)} copy(bf16[80,2048]{1,0:T(8,128)(2,1)} %shard_map.155) | data formatting | bytes 655360

commit v4 on v3

--- a/solution.py
+++ b/solution.py
@@ -453,9 +453,6 @@
     late = rows_dev - early
     table = neighbour_order(chips)
     order = [chip] + [pick(chip, [table[z][j] for z in range(chips)]) for j in range(1, chips)]
-    far = [0] + [
-        pick(chip, [abs(table[z][j] - z) for z in range(chips)]) for j in range(1, chips)
-    ]
     sends = []
     first_rows = pl.ds(0, early)
     last_rows = pl.ds(early, late)
@@ -566,11 +563,11 @@
             both_ways(2)
             launch(gc_copy(chip, 2))
 
-    def forward(at, now=None):
+    def forward(at, kinds, now=None):
         step = jnp.where(at < chip, 1, -1)
         more = jnp.where(at < chip, chip < chips - 1, chip > 0)
-        for kind in use:
-            if kind == 3:
+        for kind in kinds:
+            if kind not in use:
                 continue
             if now is None:
                 gz_wait(at, kind)
@@ -646,23 +643,54 @@
             beside,
         )
 
-    def z_sum_early(at, sender):
-        return remote(
-            partial.at[at * CORES + core, :, first_rows],
-            from_z_early.at[sender],
-            rz_send.at[at, 0],
-            rz_recv.at[sender, 0],
-            on_chip(at),
-        )
-
-    def z_sum_late(at, sender):
-        return remote(
-            partial.at[at * CORES + core, column, last_rows],
-            from_z.at[sender],
-            rz_send.at[at, 1],
-            rz_recv.at[sender, 1],
-            on_chip(at),
-        )
+    inner = (chip > 0) & (chip < chips - 1)
+    outer = (chip == 0) | (chip == chips - 1)
+
+    def z_sum(j, part):
+        at = order[j]
+        step = jnp.where(at > chip, 1, -1)
+        to = chip + step
+        slot = at
+        if chips > 2:
+            ends = outer if j == chips - 1 else False
+            if j == chips - 1:
+                to = jnp.where(outer, at, to)
+            inward = (at > 0) & (at < chips - 1) & (step < 0)
+            slot = jnp.where((to == at) & (inward | ends), chips, at)
+        mine = at * CORES + core
+        if part:
+            src, dst = partial.at[mine, column, last_rows], from_z.at[slot]
+        else:
+            src, dst = partial.at[mine, :, first_rows], from_z_early.at[slot]
+        return remote(src, dst, rz_send.at[at, part], rz_recv.at[slot, part], on_chip(to))
+
+    def z_landed(slot, part):
+        ref = (from_z if part else from_z_early).at[slot]
+        remote(
+            ref, ref, rz_send.at[chip, part], rz_recv.at[slot, part], on_chip(chip)
+        ).wait_recv()
+
+    def pass_on(j, part):
+        at = order[j]
+        mine = at * CORES + core
+
+        @pl.when(inner)
+        def _():
+            z_landed(at, part)
+            if part:
+                partial[mine, column, last_rows] = (
+                    wide(partial[mine, column, last_rows]) + wide(from_z[at])
+                ).astype(jnp.bfloat16)
+            else:
+                partial[mine, :, first_rows] = (
+                    wide(partial[mine, :, first_rows]) + wide(from_z_early[at])
+                ).astype(jnp.bfloat16)
+
+        launch(z_sum(j, part), inner)
+
+    def send_sum(j, part):
+        if j:
+            launch(z_sum(j, part), None if j == chips - 1 else outer)
 
     def wide(value):
         return value.astype(jnp.float32)
@@ -676,8 +704,7 @@
         partial[mine, :, first_rows] = (
             wide(partial[mine, :, first_rows]) + wide(from_core[at, :, first_rows])
         ).astype(jnp.bfloat16)
-        if j:
-            launch(z_sum_early(at, chip))
+        send_sum(j, 0)
 
     def sum_late(j, kind):
         at = order[j]
@@ -692,52 +719,87 @@
         if kind:
             launch(x_sum(at))
 
-    def sum_across(j):
+    def sum_across(j, now=None):
         at = order[j]
         if not late:
             return
-        x_sum(at).wait_recv()
         mine = at * CORES + core
-        partial[mine, column, last_rows] = (
-            wide(partial[mine, column, last_rows]) + wide(from_x[at])
-        ).astype(jnp.bfloat16)
-        if j:
-            launch(z_sum_late(at, chip))
-
-    def arrive(distance):
-        for j in range(distance, min(2 * distance, chips - 1) + 1):
-            if all(abs(table[z][j] - z) == distance for z in range(chips)):
-                forward(order[j])
-            else:
-                forward(order[j], far[j] == distance)
+
+        def add():
+            x_sum(at).wait_recv()
+            partial[mine, column, last_rows] = (
+                wide(partial[mine, column, last_rows]) + wide(from_x[at])
+            ).astype(jnp.bfloat16)
+
+        if now is None:
+            add()
+        else:
+            pl.when(now)(add)
+        if now is None or now is outer:
+            send_sum(j, 1)
 
     begin()
     for load in loads[3:]:
         load.wait()
-    compute_early(chip)
-    compute_late(chip, 0)
-    for j in range(chips):
+    def work(j):
         at = order[j]
-        if j == 0:
-            arrive(1)
+        compute_early(at)
+        compute_late(at, 0)
         crossed(at)
-        if j:
-            compute_early(at)
-            compute_late(at, 0)
         compute_late(at, 3)
+
+    def gather_sums(j):
         sum_early(j)
         sum_late(j, 3)
         sum_late(j, 0)
-        if j:
-            sum_across(j - 1)
-            arrive(j + 1)
+
+    compute_early(chip)
+    compute_late(chip, 0)
+    forward(order[1], (0,))
+    if chips > 2:
+        forward(order[2], (0,), inner)
+    crossed(chip)
+    compute_late(chip, 3)
+    forward(order[1], (1, 2))
+    if chips > 2:
+        forward(order[2], (1, 2), inner)
+    gather_sums(0)
+    work(1)
+    if chips > 2:
+        forward(order[2], (0,), outer)
+        forward(order[3], (0,), inner)
+        gather_sums(1)
+        sum_across(0, outer)
+        forward(order[2], (1, 2), outer)
+        forward(order[3], (1, 2), inner)
+        work(2)
+        gather_sums(2)
+        sum_across(0, inner)
+        forward(order[3], (0,), outer)
+        sum_across(1, outer)
+        forward(order[3], (1, 2), outer)
+        sum_across(2, outer)
+        work(3)
+        gather_sums(3)
+        sum_across(1, inner)
+        sum_across(2, inner)
+    else:
+        gather_sums(1)
+        sum_across(0)
+    if early:
+        for j in range(chips - 2, 0, -1):
+            pass_on(j, 0)
     sum_across(chips - 1)
+    if late:
+        for j in range(chips - 2, 0, -1):
+            pass_on(j, 1)
     mine = chip * CORES + core
+    ends = (chip, chips) if chips > 2 else (chip,)
     if early:
         total = wide(partial[mine, :, first_rows])
-        for j in range(1, chips):
-            z_sum_early(chip, order[j]).wait_recv()
-            total = total + wide(from_z_early[order[j]])
+        for slot in ends:
+            z_landed(slot, 0)
+            total = total + wide(from_z_early[slot])
         partial[mine, :, first_rows] = total.astype(jnp.bfloat16)
         last = remote(
             partial.at[mine, across, first_rows],
@@ -749,9 +811,9 @@
         launch(last)
     if late:
         total = wide(hidden[last_rows]) + wide(partial[mine, column, last_rows])
-        for j in range(1, chips):
-            z_sum_late(chip, order[j]).wait_recv()
-            total = total + wide(from_z[order[j]])
+        for slot in ends:
+            z_landed(slot, 1)
+            total = total + wide(from_z[slot])
         out_ref[last_rows] = total.astype(jnp.bfloat16)
     if early:
         last.wait_recv()
@@ -792,8 +854,8 @@
             vmem(chips, 2, *block),
             vmem(chips, late, model_width),
             vmem(max(early, 16), model_width),
-            vmem(chips, late, model_width),
-            vmem(chips, 2, max(early, 16), model_width),
+            vmem(chips + 1, late, model_width),
+            vmem(chips + 1, 2, max(early, 16), model_width),
             vmem(*block),
             vmem(*gain.shape),
             vmem(*out_w.shape),
@@ -814,7 +876,7 @@
             dma((chips + 1,)),
             dma((chips + 1,)),
             dma((chips, 2)),
-            dma((chips, 2)),
+            dma((chips + 1, 2)),
         ],
         compiler_params=pltpu.CompilerParams(
             collective_id=0, has_side_effects=True, vmem_limit_bytes=VMEM_BYTES
@@ -834,7 +896,7 @@
 def experts_fit(tokens, rows_dev, model_width):
     group, places = lax.axis_size("tp"), lax.axis_size("sp")
     chips = places // CORES
-    if group != 2 or places % CORES or chips & (chips - 1) or rows_dev % 16:
+    if group != 2 or places % CORES or chips not in (2, 4) or rows_dev % 16:
         return False
     if tokens != group * rows_dev or QK_ROPE + 2 * places > 128:
         return False

time: 108 us -> 101 us (0.935)
  Pallas kernels: 106 us -> 99.3 us
    pallas_call x1, Pallas kernels: 80.4 us -> 74.1 us  [run_experts(): pl.pallas_call(functools.partial(experts_kernel, chips, early), out_shape...]
where the time goes in v4:
time: 101 us
  Pallas kernels  99.3 us (98%)
  local copies, waits for them, and re-layouts  1.72 us (2%)
    pallas_call x1, Pallas kernels, run_experts(): pl.pallas_call(functools.partial(experts_kernel, chips, early), out_shape...  74.1 us
    pallas_call x1, Pallas kernels, run_attention(): pl.pallas_call(functools.partial(attention_kernel, chips, group), out_sha...  25.2 us

profile of v4, /device:TPU:0, one launch (start us, length us, event | category | flops | bytes accessed | tf_op | source)
XLA Modules:
  0.0 101.0 jit_solution(17823069826043995097)
XLA Ops:
  0.0 25.2 %shard_map.154 = (bf16[160,512]{1,0:T(8,128)(2,1)}, f32[16,80,1]{2,1,0:T(8,128)}) custom-call(bf16[160,512]{1,0:T(8,128)(2,1)} %refs_0_.1, bf16[512]{0:T(512)(128)(2,1)} %refs_1_.1, f32[1,128]{1,0:T(1,128)} %constant.2.clone.refs_2_, bf16[64,160]{1,0:T(8,128)(2,1)} %bitcast.13, s32[4,80]{1,0:T(4,128)} %bitcast.14, f32[4,80]{1,0:T(4,128)} %bitcast.15, ...), custom_call_target="tpu_custom_call" | custom-call | tf_op jit(solution)/shard_map/pallas_call | solution.py:366
  25.2 74.1 %shard_map.155 = bf16[80,2048]{1,0:T(8,128)(2,1)} custom-call(bf16[2,80,512]{2,1,0:T(8,128)(2,1)} %bitcast.12, f32[8,2,80,1]{3,2,1,0:T(8,128)} %bitcast.11, bf16[80,2048]{1,0:T(8,128)(2,1)} %residual_hbm.1, bf16[2048]{0:T(1024)(128)(2,1)} %gain_hbm.1, bf16[1024,2048]{1,0:T(8,128)(2,1)} %out_hbm.1, bf16[2048,512]{1,0:T(8,128)(2,1)} %bitcast.8, ...), custom_call_target="tpu_custom_call" | custom-call | tf_op jit(solution)/shard_map/pallas_call | solution.py:844
  99.3 1.7 %copy.18 = bf16[80,2048]{1,0:T(8,128)(2,1)} copy(bf16[80,2048]{1,0:T(8,128)(2,1)} %shard_map.155) | data formatting | bytes 655360

commit v5 on v4

--- a/solution.py
+++ b/solution.py
@@ -189,14 +189,9 @@
     return straight.astype(jnp.bfloat16), crossed.astype(jnp.bfloat16)
 
 
-def attention_kernel(
-    chips,
-    group,
-    *refs,
-):
-    inputs, refs = refs[:10], refs[10:]
-    out_ref, share_ref, own, gathered, queries, cosines, sines, key_turns = refs[:8]
-    held, load_sem, sems = refs[8:18], refs[18], refs[19:]
+def attention_stage(chips, group, inputs, out_ref, share_ref, refs, prefetch):
+    own, gathered, queries, cosines, sines, key_turns = refs[:6]
+    held, load_sem, sems = refs[6:16], refs[16], refs[17:]
     (
         latent_ref,
         gain_ref,
@@ -273,6 +268,7 @@
 
     for load in loads[6:]:
         load.wait()
+    prefetch()
     matrices = turn_matrices((heads_dev * QK_ROPE, heads_dev * 128), QK_ROPE)
     straight, crossed = (
         jnp.dot(query_turn_ref[...], matrix, preferred_element_type=jnp.float32)
@@ -324,11 +320,12 @@
             peaks[head], sums[head], totals[head] = peak, total, summed
         lane = lax.broadcasted_iota(jnp.int32, (width, 128), 1) - QK_ROPE
         named = (lane == place) | (lane == place + count)
-        share_ref[pl.ds(first, per_chip)] = jnp.sum(
+        share_ref[pl.ds(first // group, CORES)] = jnp.sum(
             jnp.where(named, rot.astype(jnp.float32), 0.0), axis=1, keepdims=True
-        ).reshape(per_chip, rows_dev, 1)
+        ).reshape(CORES, group, rows_dev, 1)
     for head in range(heads_dev):
-        out_ref[:, head * 128 : (head + 1) * 128] = (totals[head] / sums[head]).astype(jnp.bfloat16)
+        value = (totals[head] / sums[head]).astype(jnp.bfloat16)
+        out_ref[:, :, head * 128 : (head + 1) * 128] = value.reshape(group, rows_dev, 128)
     for copy in sends:
         copy.wait_send()
 
@@ -336,56 +333,6 @@
 def gather_sems(chips, group):
     dma = pltpu.SemaphoreType.DMA
     return [dma((chips,))] * 2 + [dma((chips, group))] * 4
-
-
-def run_attention(query, query_turn, latent, key_turn, gain, routes, route_weights, key_w, value_w):
-    group = lax.axis_size("tp")
-    chips = lax.axis_size("sp") // CORES
-    blocks = chips * CORES * group
-    tokens, latent_width = latent.shape
-    rows_dev = routes.shape[0]
-    heads_dev = query.shape[1] // PLAIN_HEAD_WIDTH
-    quarter = QK_ROPE // 4
-    freqs = theta ** (-np.arange(quarter, dtype=np.float32) / np.float32(quarter))
-    freqs = np.tile(freqs.astype(np.float32), 128 // quarter).reshape(1, 128)
-    dma = pltpu.SemaphoreType.DMA
-    whole = pl.BlockSpec(memory_space=pltpu.VMEM)
-    sent = latent_width + 128
-    arrays = (
-        latent,
-        gain,
-        jnp.asarray(freqs),
-        key_turn.T,
-        routes.T,
-        route_weights.T,
-        query_turn,
-        query,
-        key_w,
-        value_w,
-    )
-    return pl.pallas_call(
-        functools.partial(attention_kernel, chips, group),
-        out_shape=[
-            jax.ShapeDtypeStruct((tokens, heads_dev * VALUE_WIDTH), jnp.bfloat16),
-            jax.ShapeDtypeStruct((blocks, rows_dev, 1), jnp.float32),
-        ],
-        in_specs=[pl.BlockSpec(memory_space=pltpu.HBM)] * len(arrays),
-        out_specs=[whole, whole],
-        scratch_shapes=[
-            pltpu.VMEM((rows_dev, sent), jnp.bfloat16),
-            pltpu.VMEM((blocks, rows_dev, sent), jnp.bfloat16),
-            pltpu.VMEM((heads_dev, tokens, 256), jnp.bfloat16),
-            pltpu.VMEM((tokens, 128), jnp.float32),
-            pltpu.VMEM((tokens, 128), jnp.float32),
-            pltpu.VMEM((tokens, QK_ROPE), jnp.bfloat16),
-        ]
-        + [pltpu.VMEM(array.shape, array.dtype) for array in arrays]
-        + [dma((len(arrays),))]
-        + gather_sems(chips, group),
-        compiler_params=pltpu.CompilerParams(
-            collective_id=1, has_side_effects=True, vmem_limit_bytes=VMEM_BYTES
-        ),
-    )(*arrays)
 
 
 def neighbour_order(chips):
@@ -402,49 +349,38 @@
     return out
 
 
-def experts_kernel(
-    chips,
-    early,
-    attended_ref,
-    share_ref,
-    residual_hbm,
-    gain_hbm,
-    out_hbm,
-    gate_hbm,
-    up_hbm,
-    down_hbm,
-    out_ref,
-    heads,
-    hidden,
-    gathered,
-    partial,
-    from_core,
-    from_x,
-    from_x_early,
-    from_z,
-    from_z_early,
-    residual_ref,
-    gain_ref,
-    outw_ref,
-    gate_ref,
-    up_ref,
-    down_ref,
-    load_sem,
-    h_send,
-    h_recv,
-    gz_send,
-    gz_recv,
-    gx_send,
-    gx_recv,
-    gc_send,
-    gc_recv,
-    rc_send,
-    rc_recv,
-    rx_send,
-    rx_recv,
-    rz_send,
-    rz_recv,
-):
+def experts_stage(chips, early, attended_ref, share_ref, out_ref, loads, refs):
+    (
+        heads,
+        hidden,
+        gathered,
+        partial,
+        from_core,
+        from_x,
+        from_x_early,
+        from_z,
+        from_z_early,
+        residual_ref,
+        gain_ref,
+        outw_ref,
+        gate_ref,
+        up_ref,
+        down_ref,
+        h_send,
+        h_recv,
+        gz_send,
+        gz_recv,
+        gx_send,
+        gx_recv,
+        gc_send,
+        gc_recv,
+        rc_send,
+        rc_recv,
+        rx_send,
+        rx_recv,
+        rz_send,
+        rz_recv,
+    ) = refs
     place = lax.axis_index("sp")
     column = lax.axis_index("tp")
     chip, core = place // CORES, place % CORES
@@ -474,28 +410,6 @@
 
     partner = {"sp": chip * CORES + 1 - core}
     beside = {"tp": across}
-
-    barrier = pltpu.get_barrier_semaphore()
-    pl.semaphore_signal(barrier, inc=1, device_id=partner)
-    pl.semaphore_signal(barrier, inc=1, device_id=beside)
-    for j in range(1, chips):
-        pl.semaphore_signal(barrier, inc=1, device_id=on_chip((chip + j) % chips))
-    loads = [
-        pltpu.make_async_copy(src, dst, load_sem.at[i])
-        for i, (src, dst) in enumerate(
-            (
-                (residual_hbm, residual_ref),
-                (gain_hbm, gain_ref),
-                (out_hbm, outw_ref),
-                (gate_hbm, gate_ref),
-                (up_hbm, up_ref),
-                (down_hbm, down_ref),
-            )
-        )
-    ]
-    for load in loads:
-        load.start()
-    pl.semaphore_wait(barrier, chips + 1)
 
     swap = remote(attended_ref.at[across], heads.at[column], h_send, h_recv, beside)
     launch(swap)
@@ -827,26 +741,92 @@
             pl.when(when)(copy.wait_send)
 
 
-def run_experts(attended, residual, gain, shares, out_w, gate_w, up_w, down_w):
+def whole_kernel(chips, group, early, *refs):
+    inputs, refs = refs[:16], refs[16:]
+    out_ref, attended_ref, share_ref, load_sem = refs[:4]
+    first, second = refs[4:27], refs[27:]
+    loads = [
+        pltpu.make_async_copy(src, dst, load_sem.at[i])
+        for i, (src, dst) in enumerate(zip(inputs[10:], second[9:15]))
+    ]
+
+    def prefetch():
+        for load in loads:
+            load.start()
+
+    attention_stage(chips, group, inputs[:10], attended_ref, share_ref, first, prefetch)
+    experts_stage(chips, early, attended_ref, share_ref, out_ref, loads, second)
+
+
+def run_whole(
+    query,
+    query_turn,
+    latent,
+    key_turn,
+    latent_gain,
+    key_w,
+    value_w,
+    residual,
+    out_w,
+    gain,
+    gate_w,
+    up_w,
+    down_w,
+    routes,
+    route_weights,
+):
+    group = lax.axis_size("tp")
     chips = lax.axis_size("sp") // CORES
+    pairs = chips * CORES
+    tokens, latent_width = latent.shape
     rows_dev, model_width = residual.shape
-    pairs = chips * CORES
+    heads_dev = query.shape[1] // PLAIN_HEAD_WIDTH
     early = EARLY_ROWS if rows_dev > EARLY_ROWS else 0
     late = rows_dev - early
+    quarter = QK_ROPE // 4
+    freqs = theta ** (-np.arange(quarter, dtype=np.float32) / np.float32(quarter))
+    freqs = np.tile(freqs.astype(np.float32), 128 // quarter).reshape(1, 128)
     dma = pltpu.SemaphoreType.DMA
     block = (rows_dev, model_width)
-    heads = (2, rows_dev, attended.shape[1])
-    whole = pl.BlockSpec(memory_space=pltpu.VMEM)
+    heads = (group, rows_dev, heads_dev * VALUE_WIDTH)
+    sent = latent_width + 128
 
     def vmem(*shape):
         return pltpu.VMEM(shape, jnp.bfloat16)
 
+    first = (
+        latent,
+        latent_gain,
+        jnp.asarray(freqs),
+        key_turn.T,
+        routes.T,
+        route_weights.T,
+        query_turn,
+        query,
+        key_w,
+        value_w,
+    )
+    second = (residual, gain, out_w, gate_w, up_w, down_w)
     return pl.pallas_call(
-        functools.partial(experts_kernel, chips, early),
+        functools.partial(whole_kernel, chips, group, early),
         out_shape=jax.ShapeDtypeStruct(block, jnp.bfloat16),
-        in_specs=[whole] * 2 + [pl.BlockSpec(memory_space=pltpu.HBM)] * 6,
-        out_specs=whole,
+        in_specs=[pl.BlockSpec(memory_space=pltpu.HBM)] * 16,
+        out_specs=pl.BlockSpec(memory_space=pltpu.VMEM),
         scratch_shapes=[
+            vmem(*heads),
+            pltpu.VMEM((pairs, group, rows_dev, 1), jnp.float32),
+            dma((6,)),
+            vmem(rows_dev, sent),
+            vmem(pairs * group, rows_dev, sent),
+            vmem(heads_dev, tokens, 256),
+            pltpu.VMEM((tokens, 128), jnp.float32),
+            pltpu.VMEM((tokens, 128), jnp.float32),
+            vmem(tokens, QK_ROPE),
+        ]
+        + [pltpu.VMEM(array.shape, array.dtype) for array in first]
+        + [dma((len(first),))]
+        + gather_sems(chips, group)
+        + [
             vmem(*heads),
             vmem(*block),
             vmem(pairs, 2, *block),
@@ -856,13 +836,9 @@
             vmem(max(early, 16), model_width),
             vmem(chips + 1, late, model_width),
             vmem(chips + 1, 2, max(early, 16), model_width),
-            vmem(*block),
-            vmem(*gain.shape),
-            vmem(*out_w.shape),
-            vmem(*gate_w.shape),
-            vmem(*up_w.shape),
-            vmem(*down_w.shape),
-            dma((6,)),
+        ]
+        + [pltpu.VMEM(array.shape, array.dtype) for array in second]
+        + [
             dma,
             dma,
             dma((chips, 3, 2)),
@@ -881,16 +857,7 @@
         compiler_params=pltpu.CompilerParams(
             collective_id=0, has_side_effects=True, vmem_limit_bytes=VMEM_BYTES
         ),
-    )(
-        attended.reshape(heads),
-        shares.reshape(pairs, 2, rows_dev, 1),
-        residual,
-        gain,
-        out_w,
-        gate_w,
-        up_w,
-        down_w,
-    )
+    )(*first, *second)
 
 
 def experts_fit(tokens, rows_dev, model_width):
@@ -921,26 +888,22 @@
     route_weights,
 ):
     if experts_fit(latent.shape[0], *residual.shape):
-        attended, own_share = run_attention(
+        return run_whole(
             query_plain,
             query_turn,
             latent,
             key_turn,
             latent_norm_scale,
-            routes,
-            route_weights,
             plain_key_matrix,
             value_matrix,
-        )
-        return run_experts(
-            attended,
             residual,
+            out_weight,
             ffn_gain,
-            own_share,
-            out_weight,
             gate_weight[0],
             up_weight[0],
             down_weight[0],
+            routes,
+            route_weights,
         )
     tok_dev = latent.shape[0]
     heads_dev = query_plain.shape[1] // PLAIN_HEAD_WIDTH

time: 101 us -> 97.8 us (0.968)
  Pallas kernels: 99.3 us -> 96 us
    pallas_call x2 -> x1, Pallas kernels: 99.3 us -> 96 us  [run_whole(): pl.pallas_call(functools.partial(whole_kernel, chips, group, early), out_...]
where the time goes in v5:
time: 97.8 us; the launch traced here: 97.7 us
  Pallas kernels  96 us (98%)
  local copies, waits for them, and re-layouts  1.72 us (2%)
    pallas_call x1, Pallas kernels, run_whole(): pl.pallas_call(functools.partial(whole_kernel, chips, group, early), out_...  96 us

profile of v5, /device:TPU:0, one launch (start us, length us, event | category | flops | bytes accessed | tf_op | source)
XLA Modules:
  0.0 97.7 jit_solution(6702412493884402973)
XLA Ops:
  0.0 96.0 %shard_map.154 = bf16[80,2048]{1,0:T(8,128)(2,1)} custom-call(bf16[160,512]{1,0:T(8,128)(2,1)} %refs_0_.1, bf16[512]{0:T(512)(128)(2,1)} %refs_1_.1, f32[1,128]{1,0:T(1,128)} %constant.2.clone.refs_2_, bf16[64,160]{1,0:T(8,128)(2,1)} %bitcast.9, s32[4,80]{1,0:T(4,128)} %bitcast.10, f32[4,80]{1,0:T(4,128)} %bitcast.11, bf16[160,256]{1,0:T(8,128)(2,1)} %refs_6_.1, ...), custom_call_target="tpu_custom_call" | custom-call | tf_op jit(solution)/shard_map/pallas_call | solution.py:810
  96.0 1.7 %copy.18 = bf16[80,2048]{1,0:T(8,128)(2,1)} copy(bf16[80,2048]{1,0:T(8,128)(2,1)} %shard_map.154) | data formatting | bytes 655360

commit v6 on v5

--- a/solution.py
+++ b/solution.py
@@ -20,6 +20,7 @@
 slope = 1.702
 CORES = 2
 EARLY_ROWS = 32
+STRIPS = 2
 VMEM_BYTES = 60 * 2**20
 
 
@@ -189,7 +190,7 @@
     return straight.astype(jnp.bfloat16), crossed.astype(jnp.bfloat16)
 
 
-def attention_stage(chips, group, inputs, out_ref, share_ref, refs, prefetch):
+def attention_stage(chips, group, inputs, out_ref, share_ref, refs, prefetch, swap):
     own, gathered, queries, cosines, sines, key_turns = refs[:6]
     held, load_sem, sems = refs[6:16], refs[16], refs[17:]
     (
@@ -318,14 +319,15 @@
                 total = total + fade * sums[head]
                 summed = summed + fade * totals[head]
             peaks[head], sums[head], totals[head] = peak, total, summed
+            if k == chips - 1:
+                value = (summed / total).astype(jnp.bfloat16)
+                out_ref[:, :, head * 128 : (head + 1) * 128] = value.reshape(group, rows_dev, 128)
+                swap(head)
         lane = lax.broadcasted_iota(jnp.int32, (width, 128), 1) - QK_ROPE
         named = (lane == place) | (lane == place + count)
         share_ref[pl.ds(first // group, CORES)] = jnp.sum(
             jnp.where(named, rot.astype(jnp.float32), 0.0), axis=1, keepdims=True
         ).reshape(CORES, group, rows_dev, 1)
-    for head in range(heads_dev):
-        value = (totals[head] / sums[head]).astype(jnp.bfloat16)
-        out_ref[:, :, head * 128 : (head + 1) * 128] = value.reshape(group, rows_dev, 128)
     for copy in sends:
         copy.wait_send()
 
@@ -349,7 +351,7 @@
     return out
 
 
-def experts_stage(chips, early, attended_ref, share_ref, out_ref, loads, refs):
+def experts_stage(chips, early, attended_ref, out_ref, share_ref, loads, swaps, refs):
     (
         heads,
         hidden,
@@ -366,8 +368,6 @@
         gate_ref,
         up_ref,
         down_ref,
-        h_send,
-        h_recv,
         gz_send,
         gz_recv,
         gx_send,
@@ -390,6 +390,9 @@
     table = neighbour_order(chips)
     order = [chip] + [pick(chip, [table[z][j] for z in range(chips)]) for j in range(1, chips)]
     sends = []
+    strips = STRIPS if model_width % (128 * STRIPS) == 0 else 1
+    strip = model_width // strips
+    parts = [pl.ds(at * strip, strip) for at in range(strips)]
     first_rows = pl.ds(0, early)
     last_rows = pl.ds(early, late)
 
@@ -411,15 +414,19 @@
     partner = {"sp": chip * CORES + 1 - core}
     beside = {"tp": across}
 
-    swap = remote(attended_ref.at[across], heads.at[column], h_send, h_recv, beside)
-    launch(swap)
-    heads[column] = attended_ref[column]
     for load in loads[:3]:
         load.wait()
-    landed = heads.at[across]
-    remote(landed, landed, h_send, h_recv, beside).wait_recv()
-    joined = jnp.concatenate([heads[0], heads[1]], axis=1)
-    projected = jnp.dot(joined, outw_ref[...], preferred_element_type=jnp.float32)
+    half = attended_ref.shape[2]
+
+    def project(values, side):
+        rows = pl.ds(pl.multiple_of(side * half, 128), half)
+        return jnp.dot(values, outw_ref[rows, :], preferred_element_type=jnp.float32)
+
+    projected = project(attended_ref[column], column)
+    for copy in swaps:
+        copy.wait_recv()
+    projected = projected + project(heads[...], across)
+    sends.extend((copy, None) for copy in swaps)
     mixed = (residual_ref[...].astype(jnp.float32) + projected).astype(jnp.bfloat16)
     gathered[place, column] = norm_scale(mixed, gain_ref[...].reshape(1, model_width)).astype(jnp.bfloat16)
     hidden[...] = mixed
@@ -548,19 +555,19 @@
             partner,
         )
 
-    def x_sum(at):
+    def x_sum(at, n):
         return remote(
-            partial.at[at * CORES + core, across, last_rows],
-            from_x.at[at],
-            rx_send.at[at],
-            rx_recv.at[at],
+            partial.at[at * CORES + core, across, last_rows, parts[n]],
+            from_x.at[at, :, parts[n]],
+            rx_send.at[at, n],
+            rx_recv.at[at, n],
             beside,
         )
 
     inner = (chip > 0) & (chip < chips - 1)
     outer = (chip == 0) | (chip == chips - 1)
 
-    def z_sum(j, part):
+    def z_sum(j, part, n):
         at = order[j]
         step = jnp.where(at > chip, 1, -1)
         to = chip + step
@@ -573,38 +580,42 @@
             slot = jnp.where((to == at) & (inward | ends), chips, at)
         mine = at * CORES + core
         if part:
-            src, dst = partial.at[mine, column, last_rows], from_z.at[slot]
+            src = partial.at[mine, column, last_rows, parts[n]]
+            dst = from_z.at[slot, :, parts[n]]
         else:
-            src, dst = partial.at[mine, :, first_rows], from_z_early.at[slot]
-        return remote(src, dst, rz_send.at[at, part], rz_recv.at[slot, part], on_chip(to))
-
-    def z_landed(slot, part):
-        ref = (from_z if part else from_z_early).at[slot]
+            src = partial.at[mine, :, first_rows, parts[n]]
+            dst = from_z_early.at[slot, :, :, parts[n]]
+        return remote(src, dst, rz_send.at[at, part, n], rz_recv.at[slot, part, n], on_chip(to))
+
+    def z_landed(slot, part, n):
+        ref = from_z.at[slot, :, parts[n]] if part else from_z_early.at[slot, :, :, parts[n]]
         remote(
-            ref, ref, rz_send.at[chip, part], rz_recv.at[slot, part], on_chip(chip)
+            ref, ref, rz_send.at[chip, part, n], rz_recv.at[slot, part, n], on_chip(chip)
         ).wait_recv()
 
     def pass_on(j, part):
         at = order[j]
         mine = at * CORES + core
 
-        @pl.when(inner)
-        def _():
-            z_landed(at, part)
+        def add(n):
+            z_landed(at, part, n)
             if part:
-                partial[mine, column, last_rows] = (
-                    wide(partial[mine, column, last_rows]) + wide(from_z[at])
+                partial[mine, column, last_rows, parts[n]] = (
+                    wide(partial[mine, column, last_rows, parts[n]]) + wide(from_z[at, :, parts[n]])
                 ).astype(jnp.bfloat16)
             else:
-                partial[mine, :, first_rows] = (
-                    wide(partial[mine, :, first_rows]) + wide(from_z_early[at])
+                partial[mine, :, first_rows, parts[n]] = (
+                    wide(partial[mine, :, first_rows, parts[n]])
+                    + wide(from_z_early[at, :, :, parts[n]])
                 ).astype(jnp.bfloat16)
 
-        launch(z_sum(j, part), inner)
-
-    def send_sum(j, part):
+        for n in range(strips):
+            pl.when(inner)(functools.partial(add, n))
+            launch(z_sum(j, part, n), inner)
+
+    def send_sum(j, part, n):
         if j:
-            launch(z_sum(j, part), None if j == chips - 1 else outer)
+            launch(z_sum(j, part, n), None if j == chips - 1 else outer)
 
     def wide(value):
         return value.astype(jnp.float32)
@@ -618,7 +629,8 @@
         partial[mine, :, first_rows] = (
             wide(partial[mine, :, first_rows]) + wide(from_core[at, :, first_rows])
         ).astype(jnp.bfloat16)
-        send_sum(j, 0)
+        for n in range(strips):
+            send_sum(j, 0, n)
 
     def sum_late(j, kind):
         at = order[j]
@@ -631,7 +643,8 @@
             wide(partial[mine, side, last_rows]) + wide(from_core[at, side, last_rows])
         ).astype(jnp.bfloat16)
         if kind:
-            launch(x_sum(at))
+            for n in range(strips):
+                launch(x_sum(at, n))
 
     def sum_across(j, now=None):
         at = order[j]
@@ -639,18 +652,19 @@
             return
         mine = at * CORES + core
 
-        def add():
-            x_sum(at).wait_recv()
-            partial[mine, column, last_rows] = (
-                wide(partial[mine, column, last_rows]) + wide(from_x[at])
+        def add(n):
+            x_sum(at, n).wait_recv()
+            partial[mine, column, last_rows, parts[n]] = (
+                wide(partial[mine, column, last_rows, parts[n]]) + wide(from_x[at, :, parts[n]])
             ).astype(jnp.bfloat16)
 
-        if now is None:
-            add()
-        else:
-            pl.when(now)(add)
-        if now is None or now is outer:
-            send_sum(j, 1)
+        for n in range(strips):
+            if now is None:
+                add(n)
+            else:
+                pl.when(now)(functools.partial(add, n))
+            if now is None or now is outer:
+                send_sum(j, 1, n)
 
     begin()
     for load in loads[3:]:
@@ -692,11 +706,10 @@
         forward(order[3], (0,), outer)
         sum_across(1, outer)
         forward(order[3], (1, 2), outer)
-        sum_across(2, outer)
         work(3)
         gather_sums(3)
         sum_across(1, inner)
-        sum_across(2, inner)
+        sum_across(2)
     else:
         gather_sums(1)
         sum_across(0)
@@ -704,36 +717,45 @@
         for j in range(chips - 2, 0, -1):
             pass_on(j, 0)
     sum_across(chips - 1)
+    mine = chip * CORES + core
+    ends = (chip, chips) if chips > 2 else (chip,)
+
+    def last(n):
+        return remote(
+            partial.at[mine, across, first_rows, parts[n]],
+            from_x_early.at[:, parts[n]],
+            rx_send.at[chips, n],
+            rx_recv.at[chips, n],
+            beside,
+        )
+
+    if early:
+        for n in range(strips):
+            total = wide(partial[mine, :, first_rows, parts[n]])
+            for slot in ends:
+                z_landed(slot, 0, n)
+                total = total + wide(from_z_early[slot, :, :, parts[n]])
+            partial[mine, :, first_rows, parts[n]] = total.astype(jnp.bfloat16)
+            launch(last(n))
     if late:
         for j in range(chips - 2, 0, -1):
             pass_on(j, 1)
-    mine = chip * CORES + core
-    ends = (chip, chips) if chips > 2 else (chip,)
-    if early:
-        total = wide(partial[mine, :, first_rows])
-        for slot in ends:
-            z_landed(slot, 0)
-            total = total + wide(from_z_early[slot])
-        partial[mine, :, first_rows] = total.astype(jnp.bfloat16)
-        last = remote(
-            partial.at[mine, across, first_rows],
-            from_x_early,
-            rx_send.at[chips],
-            rx_recv.at[chips],
-            beside,
-        )
-        launch(last)
-    if late:
-        total = wide(hidden[last_rows]) + wide(partial[mine, column, last_rows])
-        for slot in ends:
-            z_landed(slot, 1)
-            total = total + wide(from_z[slot])
-        out_ref[last_rows] = total.astype(jnp.bfloat16)
-    if early:
-        last.wait_recv()
-        out_ref[first_rows] = (
-            wide(hidden[first_rows]) + wide(partial[mine, column, first_rows]) + wide(from_x_early[...])
-        ).astype(jnp.bfloat16)
+    for n in range(strips):
+        if late:
+            total = wide(hidden[last_rows, parts[n]]) + wide(
+                partial[mine, column, last_rows, parts[n]]
+            )
+            for slot in ends:
+                z_landed(slot, 1, n)
+                total = total + wide(from_z[slot, :, parts[n]])
+            out_ref[last_rows, parts[n]] = total.astype(jnp.bfloat16)
+        if early:
+            last(n).wait_recv()
+            out_ref[first_rows, parts[n]] = (
+                wide(hidden[first_rows, parts[n]])
+                + wide(partial[mine, column, first_rows, parts[n]])
+                + wide(from_x_early[:, parts[n]])
+            ).astype(jnp.bfloat16)
     for copy, when in sends:
         if when is None:
             copy.wait_send()
@@ -743,8 +765,23 @@
 
 def whole_kernel(chips, group, early, *refs):
     inputs, refs = refs[:16], refs[16:]
-    out_ref, attended_ref, share_ref, load_sem = refs[:4]
-    first, second = refs[4:27], refs[27:]
+    out_ref, attended_ref, share_ref, load_sem, h_send, h_recv = refs[:6]
+    first, second = refs[6:29], refs[29:]
+    column = lax.axis_index("tp")
+    swaps = []
+
+    def swap(head):
+        span = pl.ds(head * VALUE_WIDTH, VALUE_WIDTH)
+        copy = pltpu.make_async_remote_copy(
+            src_ref=attended_ref.at[1 - column, :, span],
+            dst_ref=second[0].at[:, span],
+            send_sem=h_send.at[head],
+            recv_sem=h_recv.at[head],
+            device_id={"tp": 1 - column},
+        )
+        copy.start()
+        swaps.append(copy)
+
     loads = [
         pltpu.make_async_copy(src, dst, load_sem.at[i])
         for i, (src, dst) in enumerate(zip(inputs[10:], second[9:15]))
@@ -754,8 +791,8 @@
         for load in loads:
             load.start()
 
-    attention_stage(chips, group, inputs[:10], attended_ref, share_ref, first, prefetch)
-    experts_stage(chips, early, attended_ref, share_ref, out_ref, loads, second)
+    attention_stage(chips, group, inputs[:10], attended_ref, share_ref, first, prefetch, swap)
+    experts_stage(chips, early, attended_ref, out_ref, share_ref, loads, swaps, second)
 
 
 def run_whole(
@@ -816,6 +853,8 @@
             vmem(*heads),
             pltpu.VMEM((pairs, group, rows_dev, 1), jnp.float32),
             dma((6,)),
+            dma((heads_dev,)),
+            dma((heads_dev,)),
             vmem(rows_dev, sent),
             vmem(pairs * group, rows_dev, sent),
             vmem(heads_dev, tokens, 256),
@@ -827,7 +866,7 @@
         + [dma((len(first),))]
         + gather_sems(chips, group)
         + [
-            vmem(*heads),
+            vmem(*heads[1:]),
             vmem(*block),
             vmem(pairs, 2, *block),
             vmem(pairs, 2, *block),
@@ -839,8 +878,6 @@
         ]
         + [pltpu.VMEM(array.shape, array.dtype) for array in second]
         + [
-            dma,
-            dma,
             dma((chips, 3, 2)),
             dma((chips, 3)),
             dma((chips, 2)),
@@ -849,10 +886,10 @@
             dma((chips, 4)),
             dma((chips, 4)),
             dma((chips, 4)),
-            dma((chips + 1,)),
-            dma((chips + 1,)),
-            dma((chips, 2)),
-            dma((chips + 1, 2)),
+            dma((chips + 1, STRIPS)),
+            dma((chips + 1, STRIPS)),
+            dma((chips, 2, STRIPS)),
+            dma((chips + 1, 2, STRIPS)),
         ],
         compiler_params=pltpu.CompilerParams(
             collective_id=0, has_side_effects=True, vmem_limit_bytes=VMEM_BYTES

time: 97.8 us -> 95.7 us (0.979)
  Pallas kernels: 96 us -> 93.8 us
    pallas_call x1, Pallas kernels: 96 us -> 93.8 us  [run_whole(): pl.pallas_call(functools.partial(whole_kernel, chips, group, early), out_...]
where the time goes in v6:
time: 95.7 us; the launch traced here: 95.6 us
  Pallas kernels  93.8 us (98%)
  local copies, waits for them, and re-layouts  1.72 us (2%)
    pallas_call x1, Pallas kernels, run_whole(): pl.pallas_call(functools.partial(whole_kernel, chips, group, early), out_...  93.8 us

profile of v6, /device:TPU:0, one launch (start us, length us, event | category | flops | bytes accessed | tf_op | source)
XLA Modules:
  0.0 95.6 jit_solution(4586399375984832752)
XLA Ops:
  0.0 93.8 %shard_map.154 = bf16[80,2048]{1,0:T(8,128)(2,1)} custom-call(bf16[160,512]{1,0:T(8,128)(2,1)} %refs_0_.1, bf16[512]{0:T(512)(128)(2,1)} %refs_1_.1, f32[1,128]{1,0:T(1,128)} %constant.2.clone.refs_2_, bf16[64,160]{1,0:T(8,128)(2,1)} %bitcast.9, s32[4,80]{1,0:T(4,128)} %bitcast.10, f32[4,80]{1,0:T(4,128)} %bitcast.11, bf16[160,256]{1,0:T(8,128)(2,1)} %refs_6_.1, ...), custom_call_target="tpu_custom_call" | custom-call | tf_op jit(solution)/shard_map/pallas_call | solution.py:847
  93.9 1.7 %copy.18 = bf16[80,2048]{1,0:T(8,128)(2,1)} copy(bf16[80,2048]{1,0:T(8,128)(2,1)} %shard_map.154) | data formatting | bytes 655360

commit v7 on v6

--- a/solution.py
+++ b/solution.py
@@ -697,13 +697,13 @@
         forward(order[2], (0,), outer)
         forward(order[3], (0,), inner)
         gather_sums(1)
-        sum_across(0, outer)
         forward(order[2], (1, 2), outer)
         forward(order[3], (1, 2), inner)
+        sum_across(0, outer)
         work(2)
+        forward(order[3], (0,), outer)
         gather_sums(2)
         sum_across(0, inner)
-        forward(order[3], (0,), outer)
         sum_across(1, outer)
         forward(order[3], (1, 2), outer)
         work(3)

time: 95.7 us -> 95.7 us (level)
  no operation moved by 1% of the time
where the time goes in v7:
time: 95.7 us; the launch traced here: 95.6 us
  Pallas kernels  93.8 us (98%)
  local copies, waits for them, and re-layouts  1.72 us (2%)
    pallas_call x1, Pallas kernels, run_whole(): pl.pallas_call(functools.partial(whole_kernel, chips, group, early), out_...  93.8 us

profile of v7, /device:TPU:0, one launch (start us, length us, event | category | flops | bytes accessed | tf_op | source)
XLA Modules:
  0.0 95.6 jit_solution(17453615511682100063)
XLA Ops:
  0.0 93.8 %shard_map.154 = bf16[80,2048]{1,0:T(8,128)(2,1)} custom-call(bf16[160,512]{1,0:T(8,128)(2,1)} %refs_0_.1, bf16[512]{0:T(512)(128)(2,1)} %refs_1_.1, f32[1,128]{1,0:T(1,128)} %constant.2.clone.refs_2_, bf16[64,160]{1,0:T(8,128)(2,1)} %bitcast.9, s32[4,80]{1,0:T(4,128)} %bitcast.10, f32[4,80]{1,0:T(4,128)} %bitcast.11, bf16[160,256]{1,0:T(8,128)(2,1)} %refs_6_.1, ...), custom_call_target="tpu_custom_call" | custom-call | tf_op jit(solution)/shard_map/pallas_call | solution.py:847
  93.8 1.7 %copy.18 = bf16[80,2048]{1,0:T(8,128)(2,1)} copy(bf16[80,2048]{1,0:T(8,128)(2,1)} %shard_map.154) | data formatting | bytes 655360
